TPU v7x, 32 devices: a whole 2x2x4 slice. The times are simulated.
32 devices in a mesh: grp: 2 (over y), sp: 4 (over z), tp: 4 (over x, core).
Axes of the slice: x: 2, y: 2, z: 4, core: 2. Of those that a mesh axis runs over, the one named last changes fastest.
Arguments:
- residual: bfloat16 [2048, 2048], P(('grp', 'sp')), parts along dimension 0, may hold values from -6 to 6
- queries: bfloat16 [2048, 1024], P(('grp', 'sp'), 'tp'), parts along dimension 0, may hold values from -400 to 400
- keys: bfloat16 [2048, 1024], P(('grp', 'sp'), 'tp'), parts along dimension 0, may hold values from -8 to 8
- values: bfloat16 [2048, 1024], P(('grp', 'sp'), 'tp'), parts along dimension 0, may hold values from -6 to 6
- log_gates: float32 [2048, 16], P(('grp', 'sp'), 'tp'), parts along dimension 0, may hold values from -126 to 0, as said below
- w_out: bfloat16 [1024, 2048], P('tp'), may hold values from -0.75 to 0.75
- norm_gain: float32 [2048], replicated, may hold values from 0.1 to 1.9
- w_gate: bfloat16 [2048, 5632], P('sp', 'tp'), may hold values from -0.125 to 0.125
- w_up: bfloat16 [2048, 5632], P('sp', 'tp'), may hold values from -0.125 to 0.125
- w_down: bfloat16 [5632, 2048], P('tp', 'sp'), may hold values from -0.078125 to 0.078125
Outputs:
- output: bfloat16 [2048, 2048], P(('grp', 'sp', 'tp')), parts along dimension 0
There are 2 independent parts, one for each index of `grp`. A program takes and returns all parts, laid end to end along the dimension named above; an argument that names none is the same for every part. Nothing has to cross between parts.
Inputs may be any that keep to these rules, and one draw needn't show every extreme that they name: `log_gates`: never rises along positions.
All inputs are finite; a program needn't handle non-finite values.
Results may differ from a plain program's by a relative error of at most 0.014.
Values may be sent and summed in bfloat16 or wider, within the bound.
A program may use at most 128 MiB of HBM per device.

v0:
```python
import functools
import math

import jax
import jax.numpy as jnp
from jax import lax
from jax.experimental import pallas as pl
from jax.experimental.pallas import tpu as pltpu
from jax.sharding import PartitionSpec as P


def normalize(rows_in, gain):
    floats = rows_in.astype(jnp.float32)
    scaled = floats * lax.rsqrt(jnp.mean(floats * floats, axis=-1, keepdims=True) + 1e-06)
    return (scaled * gain).astype(jnp.bfloat16)


def attend(queries, keys, values, log_gates):
    row_count = queries.shape[0]
    head_count = log_gates.shape[1]
    head_width = queries.shape[1] // head_count
    score_scale = head_width ** (-0.5)
    first_row = lax.axis_index("sp") * row_count
    query_heads = queries.reshape(row_count, head_count, head_width)
    query_gates = log_gates.T
    query_positions = first_row + jnp.arange(row_count, dtype=jnp.int32)
    initial = (
        jnp.full((head_count, row_count), -1e30, jnp.float32),
        jnp.zeros((head_count, row_count), jnp.float32),
        jnp.zeros((head_count, row_count, head_width), jnp.float32),
    )
    carried = initial
    key_piece = lax.all_gather(keys.astype(jnp.float32), "sp", axis=0, tiled=True).astype(
        jnp.bfloat16
    )
    value_piece = lax.all_gather(values.astype(jnp.float32), "sp", axis=0, tiled=True).astype(
        jnp.bfloat16
    )
    gate_piece = lax.all_gather(log_gates, "sp", axis=0, tiled=True)
    length = key_piece.shape[0]
    block_rows = math.gcd(length, 2048)
    block_count = length // block_rows
    key_blocks = key_piece.reshape(block_count, block_rows, head_count, head_width)
    value_blocks = value_piece.reshape(block_count, block_rows, head_count, head_width)
    gate_blocks = gate_piece.reshape(block_count, block_rows, head_count)
    offsets = jnp.arange(block_count, dtype=jnp.int32) * block_rows

    def one_block(state, inputs):
        current_key_block, value_block, gate_block, offset = inputs

        def work(current):
            running_max, running_sum, accumulated = current
            scores = (
                jnp.einsum(
                    "qhd,khd->hqk",
                    query_heads,
                    current_key_block,
                    preferred_element_type=jnp.float32,
                )
                * score_scale
            )
            scores = scores + query_gates[:, :, None] - gate_block.T[:, None, :]
            key_positions = offset + jnp.arange(block_rows, dtype=jnp.int32)
            causal = (query_positions[:, None] >= key_positions[None, :])[None]
            scores = jnp.where(causal, scores, -1e30)
            new_max = jnp.maximum(running_max, jnp.max(scores, axis=-1))
            weights = jnp.where(causal, jnp.exp(scores - new_max[:, :, None]), 0.0)
            rescale = jnp.exp(running_max - new_max)
            running_sum = running_sum * rescale + jnp.sum(weights, axis=-1)
            product = jnp.einsum(
                "hqk,khd->hqd",
                weights.astype(jnp.bfloat16),
                value_block,
                preferred_element_type=jnp.float32,
            )
            accumulated = accumulated * rescale[:, :, None] + product
            return (new_max, running_sum, accumulated)

        state = lax.cond(offset <= first_row + row_count - 1, work, lambda current: current, state)
        return (state, None)

    carried, _ = lax.scan(one_block, carried, (key_blocks, value_blocks, gate_blocks, offsets))
    running_max, running_sum, accumulated = carried
    attended = accumulated / running_sum[:, :, None]
    return (
        attended.transpose(1, 0, 2).reshape(row_count, head_count * head_width).astype(jnp.bfloat16)
    )


def body(residual, queries, keys, values, log_gates, w_out, norm_gain, w_gate, w_up, w_down):
    attended = attend(queries, keys, values, log_gates)
    row_count = attended.shape[0]
    per_device = row_count // lax.axis_size("tp")
    my_first = lax.axis_index("tp") * per_device
    projected = lax.psum(
        jnp.dot(attended, w_out, preferred_element_type=jnp.float32).astype(jnp.bfloat16), "tp"
    ).astype(jnp.float32)
    mixed_all = (residual.astype(jnp.float32) + projected).astype(jnp.bfloat16)
    normed_all = normalize(mixed_all, norm_gain)
    mixed = lax.dynamic_slice_in_dim(mixed_all, my_first, per_device, 0)
    gate_whole = lax.all_gather(w_gate, "sp", axis=0, tiled=True)
    up_whole = lax.all_gather(w_up, "sp", axis=0, tiled=True)
    down_whole = lax.all_gather(w_down, "sp", axis=1, tiled=True)
    gate_proj = jnp.dot(normed_all, gate_whole, preferred_element_type=jnp.float32)
    up_proj = jnp.dot(normed_all, up_whole, preferred_element_type=jnp.float32)
    hidden = (jax.nn.silu(gate_proj) * up_proj).astype(jnp.bfloat16)
    down_sum = lax.psum_scatter(
        jnp.dot(hidden, down_whole, preferred_element_type=jnp.float32).astype(jnp.bfloat16),
        "tp",
        scatter_dimension=0,
        tiled=True,
    ).astype(jnp.float32)
    summed = mixed.astype(jnp.float32) + 0.5 * down_sum
    scaled = summed * lax.rsqrt(jnp.mean(summed * summed, axis=-1, keepdims=True) + 1e-06)
    return scaled.astype(jnp.bfloat16)


MESH = pl.DeviceIdType.MESH


def send(src, dst, sems, index, target):
    return pltpu.make_async_remote_copy(
        src_ref=src,
        dst_ref=dst,
        send_sem=sems.at[(0, *index)],
        recv_sem=sems.at[(1, *index)],
        device_id=target,
        device_id_type=MESH,
    )


def layer_kernel(
    n, tp, chunk,
    q_ref, k_ref, v_ref, g_ref, gt_ref, residual_ref, w_out_ref, gain_ref, wg_ref, wu_ref, wd_ref,
    out_ref,
    k_all, v_all, gt_all, att, proj, pc_buf, px_send, px_buf, mixed, normed,
    wg_all, wu_all, wd_all, hid, part, c_buf, x_send, x_buf, z_send, z_buf,
    kv_sems, w_sems, y_sems, pc_sems, px_sems, nz_sems, nx_sems, nc_sems, c_sems, x_sems, z_sems, o_sems,
):
    me = lax.axis_index("sp")
    t = lax.axis_index("tp")
    g = lax.axis_index("grp")
    x, c = t // 2, t % 2
    nx = tp // 2
    mate = x * 2 + (1 - c)
    rows = q_ref.shape[0]
    sub = rows // tp
    width = residual_ref.shape[1]
    heads = g_ref.shape[1]
    head = q_ref.shape[1] // heads
    depth = wg_ref.shape[0]
    ff = wg_ref.shape[1]
    half = depth // 2
    dcols = wd_ref.shape[1]
    dhalf = dcols // 2

    def there(d):
        return lax.rem(me + d, n)

    def origin(d):
        return lax.rem(me + n - d, n)

    def across(dx):
        return lax.rem(x + dx, nx)

    barrier = pltpu.get_barrier_semaphore()
    for d in range(1, n):
        pl.semaphore_signal(barrier, inc=1, device_id={"sp": there(d)}, device_id_type=MESH)
    for dx in range(1, nx):
        pl.semaphore_signal(
            barrier, inc=1, device_id={"tp": across(dx) * 2 + c}, device_id_type=MESH
        )
    pl.semaphore_signal(barrier, inc=1, device_id={"tp": mate}, device_id_type=MESH)
    pl.semaphore_signal(barrier, inc=1, device_id={"grp": 1 - g}, device_id_type=MESH)
    pl.semaphore_wait(barrier, n - 1 + nx - 1 + 2)

    def kv_copies(d):
        target = {"sp": lax.rem(me + 1, n)}
        own = (k_ref, v_ref, gt_ref)
        held = (k_all, v_all, gt_all)
        return [
            send(
                own[i] if d == 1 else held[i].at[d - 2], held[i].at[d - 1], kv_sems, (d - 1, i), target
            )
            for i in range(3)
        ]

    @pl.when(me + 1 < n)
    def _():
        for copy in kv_copies(1):
            copy.start()

    last = ff - (n - 1) * chunk
    my_rows = pl.ds(pl.multiple_of(g * half, half), half)
    my_cols = pl.ds(pl.multiple_of(g * dhalf, dhalf), dhalf)

    def w_copies(d, size):
        j = there(d)
        place = pl.ds(pl.multiple_of(jnp.minimum(j * chunk, ff - size), 128), size)
        target = {"sp": j}
        return (
            send(wg_ref.at[my_rows, place], wg_all.at[d, my_rows, :size], w_sems, (d - 1, 0), target),
            send(wu_ref.at[my_rows, place], wu_all.at[d, my_rows, :size], w_sems, (d - 1, 1), target),
            send(wd_ref.at[place, my_cols], wd_all.at[d, :size, my_cols], w_sems, (d - 1, 2), target),
        )

    def y_copies(d, size):
        target = {"grp": 1 - g}
        gate = wg_all.at[d, my_rows, :size]
        up = wu_all.at[d, my_rows, :size]
        down = wd_all.at[d, :size, my_cols]
        return (
            send(gate, gate, y_sems, (d - 1, 0), target),
            send(up, up, y_sems, (d - 1, 1), target),
            send(down, down, y_sems, (d - 1, 2), target),
        )

    def by_window(owner, work):
        pl.when(owner < n - 1)(lambda: work(chunk))
        pl.when(owner == n - 1)(lambda: work(last))

    def start_weights(d):
        def work(size):
            for copy in w_copies(d, size):
                copy.start()

        by_window(there(d), work)

    def pass_weights(d):
        def work(size):
            for copy, forward in zip(w_copies(d, size), y_copies(d, size)):
                copy.wait_recv()
                forward.start()

        by_window(me, work)

    for d in range(1, n):

        @pl.when(me + d >= n)
        def _(d=d):
            start_weights(d)

    def own_copies(size):
        mine = pl.ds(pl.multiple_of(jnp.minimum(me * chunk, ff - size), 128), size)
        return (
            pltpu.make_async_copy(wg_ref.at[:, mine], wg_all.at[0, :, :size], o_sems.at[0]),
            pltpu.make_async_copy(wu_ref.at[:, mine], wu_all.at[0, :, :size], o_sems.at[1]),
            pltpu.make_async_copy(wd_ref.at[mine, :], wd_all.at[0, :size, :], o_sems.at[2]),
        )

    def own_weights(size):
        for copy in own_copies(size):
            copy.start()
        if size < chunk:
            for d in range(n):
                wg_all[d, :, size:] = jnp.zeros((depth, chunk - size), jnp.bfloat16)
                wu_all[d, :, size:] = jnp.zeros((depth, chunk - size), jnp.bfloat16)
                wd_all[d, size:, :] = jnp.zeros((chunk - size, dcols), jnp.bfloat16)

    by_window(me, own_weights)

    for d in range(1, n):
        if d == n - 1:
            for e in range(1, n):

                @pl.when(me + e < n)
                def _(e=e):
                    start_weights(e)

        @pl.when(me >= d)
        def _(d=d):
            arrived = kv_copies(d)
            forwards = kv_copies(d + 1) if d + 1 < n else [None] * 3
            for copy, forward in zip(arrived, forwards):
                copy.wait_recv()
                if forward is not None:
                    pl.when(me + 1 < n)(forward.start)

        @pl.when(me < d)
        def _(d=d):
            k_all[d - 1] = jnp.zeros_like(k_ref)
            v_all[d - 1] = jnp.zeros_like(v_ref)
            gt_all[d - 1] = jnp.zeros_like(gt_ref)

    pair = 128 // head
    lane = lax.broadcasted_iota(jnp.int32, (rows, 128), 1)
    causal = lax.broadcasted_iota(jnp.int32, (rows, rows), 0) >= lax.broadcasted_iota(
        jnp.int32, (rows, rows), 1
    )
    contract = (((1,), (1,)), ((), ()))
    for p in range(heads // pair):
        cols = slice(p * 128, (p + 1) * 128)
        q_pair = q_ref[:, cols]
        joined = jnp.zeros((rows, 128), jnp.float32)
        for i in range(pair):
            h = p * pair + i
            inside = (lane >= i * head) & (lane < (i + 1) * head)
            q_head = jnp.where(inside, q_pair, jnp.zeros_like(q_pair))
            g_query = g_ref[:, h : h + 1]
            scores = []
            for d in range(n):
                k_pair = k_ref[:, cols] if d == 0 else k_all[d - 1, :, cols]
                g_key = gt_ref[h : h + 1, :] if d == 0 else gt_all[d - 1, h : h + 1, :]
                score = (
                    lax.dot_general(q_head, k_pair, contract, preferred_element_type=jnp.float32)
                    * head ** (-0.5)
                    + g_query
                    - g_key
                )
                allowed = causal if d == 0 else (jnp.zeros((rows, rows), jnp.int32) + me) >= d
                scores.append(jnp.where(allowed, score, -1e30))
            peak = functools.reduce(
                jnp.maximum, [jnp.max(score, axis=-1, keepdims=True) for score in scores]
            )
            total = jnp.zeros((rows, 1), jnp.float32)
            summed = jnp.zeros((rows, 128), jnp.float32)
            for d in range(n):
                v_pair = v_ref[:, cols] if d == 0 else v_all[d - 1, :, cols]
                weight = jnp.exp(scores[d] - peak)
                total += jnp.sum(weight, axis=-1, keepdims=True)
                summed += jnp.dot(
                    weight.astype(jnp.bfloat16), v_pair, preferred_element_type=jnp.float32
                )
            joined = jnp.where(inside, summed / total, joined)
        att[:, cols] = joined.astype(jnp.bfloat16)

    pass_weights(1)
    for k in range(width // 512):
        cols = slice(k * 512, (k + 1) * 512)
        proj[:, cols] = jnp.dot(
            att[...], w_out_ref[:, cols], preferred_element_type=jnp.float32
        ).astype(jnp.bfloat16)

    def block(index):
        return pl.ds(pl.multiple_of(index * sub, sub), sub)

    pc = [
        send(proj.at[block(across(dx) * 2 + 1 - c)], pc_buf.at[dx], pc_sems, (dx,), {"tp": mate})
        for dx in range(nx)
    ]
    for copy in pc:
        copy.start()
    px = [
        send(px_send.at[dx], px_buf.at[dx], px_sems, (dx,), {"tp": across(dx) * 2 + c})
        for dx in range(nx)
    ]
    for dx in range(1, nx):
        pc[dx].wait_recv()
        px_send[dx] = (
            proj[block(across(dx) * 2 + c), :].astype(jnp.float32) + pc_buf[dx].astype(jnp.float32)
        ).astype(jnp.bfloat16)
        px[dx].start()
    if n > 2:
        pass_weights(2)
    pc[0].wait_recv()
    acc = proj[block(t), :].astype(jnp.float32) + pc_buf[0].astype(jnp.float32)
    for dx in range(1, nx):
        px[dx].wait_recv()
        acc += px_buf[dx].astype(jnp.float32)
    mix = (residual_ref[block(t), :].astype(jnp.float32) + acc).astype(jnp.bfloat16)
    mixed[...] = mix
    floats = mix.astype(jnp.float32)
    scale = lax.rsqrt(jnp.mean(floats * floats, axis=-1, keepdims=True) + 1e-06)
    normed[me, block(t), :] = (floats * scale * gain_ref[...]).astype(jnp.bfloat16)

    own = normed.at[me, block(t)]
    nz = [send(own, own, nz_sems, (d,), {"sp": there(d)}) for d in range(n)]
    for d in range(1, n):
        nz[d].start()

    def spread(d):
        piece = normed.at[origin(d), block(t)]
        copies = [send(piece, piece, nc_sems, (d, 0), {"tp": mate})]
        for dx in range(1, nx):
            copies.append(send(piece, piece, nx_sems, (d, dx), {"tp": across(dx) * 2 + c}))
        return copies

    def relay(d, dx):
        piece = normed.at[origin(d), block(lax.rem(x + nx - dx, nx) * 2 + c)]
        return send(piece, piece, nc_sems, (d, dx), {"tp": mate})

    spreads = [spread(d) for d in range(n)]
    for copy in spreads[0]:
        copy.start()
    for d in range(3, n):
        pass_weights(d)

    def relay_all(d):
        for dx in range(1, nx):
            spreads[d][dx].wait_recv()
            relay(d, dx).start()

    relay_all(0)
    for d in range(1, n):
        nz[d].wait_recv()
        for copy in spreads[d]:
            copy.start()
        if d > 1:
            relay_all(d - 1)

    def y_arrived(size):
        for copy in own_copies(size):
            copy.wait()
        for d in range(1, n):
            for copy in y_copies(d, size):
                copy.wait_recv()

    by_window(me, y_arrived)

    def c_copy(d, dx):
        j = origin(d)
        return send(
            part.at[j, block(across(dx) * 2 + 1 - c)], c_buf.at[d, dx], c_sems, (d, dx), {"tp": mate}
        )

    def feed(d):
        j = origin(d)
        spreads[d][0].wait_recv()
        for dx in range(1, nx):
            relay(d, dx).wait_recv()
        gate = jnp.zeros((rows, chunk), jnp.float32)
        up = jnp.zeros((rows, chunk), jnp.float32)
        for e in range(n):
            piece = normed[j, :, pl.ds(pl.multiple_of(origin(e) * depth, depth), depth)]
            gate += jnp.dot(piece, wg_all[e], preferred_element_type=jnp.float32)
            up += jnp.dot(piece, wu_all[e], preferred_element_type=jnp.float32)
        hid[...] = (gate / (1.0 + jnp.exp(-gate)) * up).astype(jnp.bfloat16)
        for e in range(n):
            part[j, :, pl.ds(pl.multiple_of(origin(e) * dcols, dcols), dcols)] = jnp.dot(
                hid[...], wd_all[e], preferred_element_type=jnp.float32
            ).astype(jnp.bfloat16)
        for dx in range(nx):
            c_copy(d, dx).start()

    def x_copy(d, dx):
        return send(x_send.at[d, dx], x_buf.at[d, dx], x_sems, (d, dx), {"tp": across(dx) * 2 + c})

    def z_copy(d):
        return send(z_send.at[d], z_buf.at[d], z_sems, (d,), {"sp": origin(d)})

    def over_x(d):
        for dx in range(1, nx):
            c_copy(d, dx).wait_recv()
            x_send[d, dx] = (
                part[origin(d), block(across(dx) * 2 + c), :].astype(jnp.float32)
                + c_buf[d, dx].astype(jnp.float32)
            ).astype(jnp.bfloat16)
            x_copy(d, dx).start()

    def over_z(d):
        c_copy(d, 0).wait_recv()
        acc = part[origin(d), block(t), :].astype(jnp.float32) + c_buf[d, 0].astype(jnp.float32)
        for dx in range(1, nx):
            x_copy(d, dx).wait_recv()
            acc += x_buf[d, dx].astype(jnp.float32)
        if d != 0:
            z_send[d] = acc.astype(jnp.bfloat16)
            z_copy(d).start()
        return acc

    for d in range(n):
        if d == n - 1:
            relay_all(d)
        feed(d)
        if d > 0:
            over_x(d - 1)
        if d > 2:
            over_z(d - 2)
    over_x(n - 1)
    for d in range(max(1, n - 2), n):
        over_z(d)
    acc = over_z(0)
    for d in range(1, n):
        z_copy(d).wait_recv()
        acc += z_buf[d].astype(jnp.float32)
    summed = mixed[...].astype(jnp.float32) + 0.5 * acc
    scale = lax.rsqrt(jnp.mean(summed * summed, axis=-1, keepdims=True) + 1e-06)
    out_ref[...] = (summed * scale).astype(jnp.bfloat16)

    for copy in pc:
        copy.wait_send()
    for dx in range(1, nx):
        px[dx].wait_send()
    for d in range(n):
        for copy in spreads[d]:
            copy.wait_send()
        for dx in range(1, nx):
            relay(d, dx).wait_send()
            x_copy(d, dx).wait_send()
        for dx in range(nx):
            c_copy(d, dx).wait_send()
    for d in range(1, n):
        nz[d].wait_send()
        z_copy(d).wait_send()

        def w_sent(size, d=d):
            for copy in w_copies(d, size):
                copy.wait_send()

        def y_sent(size, d=d):
            for copy in y_copies(d, size):
                copy.wait_send()

        by_window(there(d), w_sent)
        by_window(me, y_sent)

        @pl.when((me >= d - 1) & (me + 1 < n))
        def _(d=d):
            for copy in kv_copies(d):
                copy.wait_send()


def fused_body(residual, queries, keys, values, log_gates, w_out, norm_gain, w_gate, w_up, w_down):
    n, tp = lax.axis_size("sp"), lax.axis_size("tp")
    rows, width = residual.shape
    sub = rows // tp
    nx = tp // 2
    heads = log_gates.shape[1]
    depth, ff = w_gate.shape
    dcols = w_down.shape[1]
    chunk = window(ff, n)
    gates_t = jnp.pad(log_gates.T, ((0, -heads % 8), (0, 0)))
    bf16, f32 = jnp.bfloat16, jnp.float32
    shapes = [
        ((n - 1, *keys.shape), bf16),
        ((n - 1, *values.shape), bf16),
        ((n - 1, *gates_t.shape), f32),
        (queries.shape, bf16),
        ((rows, width), bf16),
        ((nx, sub, width), bf16),
        ((nx, sub, width), bf16),
        ((nx, sub, width), bf16),
        ((sub, width), bf16),
        ((n, rows, width), bf16),
        ((n, depth, chunk), bf16),
        ((n, depth, chunk), bf16),
        ((n, chunk, dcols), bf16),
        ((rows, chunk), bf16),
        ((n, rows, width), bf16),
        ((n, nx, sub, width), bf16),
        ((n, nx, sub, width), bf16),
        ((n, nx, sub, width), bf16),
        ((n, sub, width), bf16),
        ((n, sub, width), bf16),
    ]
    sems = [
        (2, n - 1, 3),
        (2, n - 1, 3),
        (2, n - 1, 3),
        (2, nx),
        (2, nx),
        (2, n),
        (2, n, nx),
        (2, n, nx),
        (2, n, nx),
        (2, n, nx),
        (2, n),
        (3,),
    ]
    return pl.pallas_call(
        functools.partial(layer_kernel, n, tp, chunk),
        out_shape=jax.ShapeDtypeStruct((sub, width), bf16),
        in_specs=[pl.BlockSpec(memory_space=pltpu.VMEM)] * 8
        + [pl.BlockSpec(memory_space=pl.ANY)] * 3,
        out_specs=pl.BlockSpec(memory_space=pltpu.VMEM),
        scratch_shapes=[pltpu.VMEM(shape, dtype) for shape, dtype in shapes]
        + [pltpu.SemaphoreType.DMA(shape) for shape in sems],
        compiler_params=pltpu.CompilerParams(
            collective_id=0, has_side_effects=True, vmem_limit_bytes=60 * 1024 * 1024
        ),
    )(
        queries, keys, values, log_gates, gates_t, residual, w_out, norm_gain[None, :],
        w_gate, w_up, w_down,
    )


def window(ff, n):
    return -(-ff // (n * 128)) * 128


def fits(mesh, shapes):
    residual, queries, gates, gate = shapes
    n, tp, grp = mesh.shape["sp"], mesh.shape["tp"], mesh.shape["grp"]
    ff = gate[1] // tp
    heads = gates[1] // tp
    head = queries[1] // gates[1]
    rows = residual[0] // (grp * n)
    return (
        grp == 2
        and 2 <= n <= 4
        and tp % 2 == 0
        and ff % 128 == 0
        and window(ff, n) * (n - 1) < ff
        and 128 % head == 0
        and (heads * head) % 128 == 0
        and rows % (16 * tp) == 0
        and rows * n * residual[1] <= 1 << 21
    )


def solution(mesh):
    in_specs = (
        P(("grp", "sp"), None),
        P(("grp", "sp"), "tp"),
        P(("grp", "sp"), "tp"),
        P(("grp", "sp"), "tp"),
        P(("grp", "sp"), "tp"),
        P("tp", None),
        P(),
        P("sp", "tp"),
        P("sp", "tp"),
        P("tp", "sp"),
    )
    out_specs = P(("grp", "sp", "tp"), None)

    def layer(*args):
        residual, queries, _, _, log_gates, _, _, w_gate, _, _ = args
        shapes = (residual.shape, queries.shape, log_gates.shape, w_gate.shape)
        chosen = fused_body if fits(mesh, shapes) else body
        return jax.shard_map(
            chosen, mesh=mesh, in_specs=in_specs, out_specs=out_specs, check_vma=False
        )(*args)

    return layer
```

profile of v0, /device:TPU:0, one launch (start us, length us, event | category | flops | bytes accessed | tf_op | source)
XLA Modules:
  0.0 144.5 jit_solution(17174644291510654811)
XLA Ops:
  0.0 1.3 pad.4.gt_ref
  1.3 1.5 %copy.11.g_ref = f32[256,4]{1,0:T(8,128)} copy(f32[256,4]{0,1:T(4,128)} %param.14) | data formatting | bytes 8192 | tf_op args[4]
  2.8 140.1 %shard_map.100 = bf16[64,2048]{1,0:T(8,128)(2,1)} custom-call(bf16[256,256]{1,0:T(8,128)(2,1)} %q_ref.1, bf16[256,256]{1,0:T(8,128)(2,1)} %k_ref.1, bf16[256,256]{1,0:T(8,128)(2,1)} %v_ref.1, f32[256,4]{1,0:T(8,128)} %copy.11.g_ref, f32[8,256]{1,0:T(8,128)} %pad.4.gt_ref, bf16[256,2048]{1,0:T(8,128)(2,1)} %residual_ref.1, bf16[256,2048]{1,0:T(8,128)(2,1)} %w_out_ref.1, ...), custom_call_target="tpu_custom_call" | custom-call | tf_op jit(solution)/shard_map/pallas_call | solution.py:560
  142.8 1.7 %copy.13 = bf16[64,2048]{1,0:T(8,128)(2,1)} copy(bf16[64,2048]{1,0:T(8,128)(2,1)} %shard_map.100) | data formatting | bytes 524288
where the time goes:
time: 146 us; the launch traced here: 145 us
  Pallas kernels  140 us (96%)
  local copies, waits for them, and re-layouts  4.43 us (3%)
    pallas_call x1, Pallas kernels, fused_body(): pl.pallas_call(functools.partial(layer_kernel, n, tp, chunk), out_shape=j...  140 us
    unnamed x2, local copies, waits for them, and re-layouts  3.15 us

commit v1 on v0

v1 whole, which is shorter than its diff:
```python
import functools
import math

import jax
import jax.numpy as jnp
from jax import lax
from jax.experimental import pallas as pl
from jax.experimental.pallas import tpu as pltpu
from jax.sharding import PartitionSpec as P


def normalize(rows_in, gain):
    floats = rows_in.astype(jnp.float32)
    scaled = floats * lax.rsqrt(jnp.mean(floats * floats, axis=-1, keepdims=True) + 1e-06)
    return (scaled * gain).astype(jnp.bfloat16)


def attend(queries, keys, values, log_gates):
    row_count = queries.shape[0]
    head_count = log_gates.shape[1]
    head_width = queries.shape[1] // head_count
    score_scale = head_width ** (-0.5)
    first_row = lax.axis_index("sp") * row_count
    query_heads = queries.reshape(row_count, head_count, head_width)
    query_gates = log_gates.T
    query_positions = first_row + jnp.arange(row_count, dtype=jnp.int32)
    initial = (
        jnp.full((head_count, row_count), -1e30, jnp.float32),
        jnp.zeros((head_count, row_count), jnp.float32),
        jnp.zeros((head_count, row_count, head_width), jnp.float32),
    )
    carried = initial
    key_piece = lax.all_gather(keys.astype(jnp.float32), "sp", axis=0, tiled=True).astype(
        jnp.bfloat16
    )
    value_piece = lax.all_gather(values.astype(jnp.float32), "sp", axis=0, tiled=True).astype(
        jnp.bfloat16
    )
    gate_piece = lax.all_gather(log_gates, "sp", axis=0, tiled=True)
    length = key_piece.shape[0]
    block_rows = math.gcd(length, 2048)
    block_count = length // block_rows
    key_blocks = key_piece.reshape(block_count, block_rows, head_count, head_width)
    value_blocks = value_piece.reshape(block_count, block_rows, head_count, head_width)
    gate_blocks = gate_piece.reshape(block_count, block_rows, head_count)
    offsets = jnp.arange(block_count, dtype=jnp.int32) * block_rows

    def one_block(state, inputs):
        current_key_block, value_block, gate_block, offset = inputs

        def work(current):
            running_max, running_sum, accumulated = current
            scores = (
                jnp.einsum(
                    "qhd,khd->hqk",
                    query_heads,
                    current_key_block,
                    preferred_element_type=jnp.float32,
                )
                * score_scale
            )
            scores = scores + query_gates[:, :, None] - gate_block.T[:, None, :]
            key_positions = offset + jnp.arange(block_rows, dtype=jnp.int32)
            causal = (query_positions[:, None] >= key_positions[None, :])[None]
            scores = jnp.where(causal, scores, -1e30)
            new_max = jnp.maximum(running_max, jnp.max(scores, axis=-1))
            weights = jnp.where(causal, jnp.exp(scores - new_max[:, :, None]), 0.0)
            rescale = jnp.exp(running_max - new_max)
            running_sum = running_sum * rescale + jnp.sum(weights, axis=-1)
            product = jnp.einsum(
                "hqk,khd->hqd",
                weights.astype(jnp.bfloat16),
                value_block,
                preferred_element_type=jnp.float32,
            )
            accumulated = accumulated * rescale[:, :, None] + product
            return (new_max, running_sum, accumulated)

        state = lax.cond(offset <= first_row + row_count - 1, work, lambda current: current, state)
        return (state, None)

    carried, _ = lax.scan(one_block, carried, (key_blocks, value_blocks, gate_blocks, offsets))
    running_max, running_sum, accumulated = carried
    attended = accumulated / running_sum[:, :, None]
    return (
        attended.transpose(1, 0, 2).reshape(row_count, head_count * head_width).astype(jnp.bfloat16)
    )


def body(residual, queries, keys, values, log_gates, w_out, norm_gain, w_gate, w_up, w_down):
    attended = attend(queries, keys, values, log_gates)
    row_count = attended.shape[0]
    per_device = row_count // lax.axis_size("tp")
    my_first = lax.axis_index("tp") * per_device
    projected = lax.psum(
        jnp.dot(attended, w_out, preferred_element_type=jnp.float32).astype(jnp.bfloat16), "tp"
    ).astype(jnp.float32)
    mixed_all = (residual.astype(jnp.float32) + projected).astype(jnp.bfloat16)
    normed_all = normalize(mixed_all, norm_gain)
    mixed = lax.dynamic_slice_in_dim(mixed_all, my_first, per_device, 0)
    gate_whole = lax.all_gather(w_gate, "sp", axis=0, tiled=True)
    up_whole = lax.all_gather(w_up, "sp", axis=0, tiled=True)
    down_whole = lax.all_gather(w_down, "sp", axis=1, tiled=True)
    gate_proj = jnp.dot(normed_all, gate_whole, preferred_element_type=jnp.float32)
    up_proj = jnp.dot(normed_all, up_whole, preferred_element_type=jnp.float32)
    hidden = (jax.nn.silu(gate_proj) * up_proj).astype(jnp.bfloat16)
    down_sum = lax.psum_scatter(
        jnp.dot(hidden, down_whole, preferred_element_type=jnp.float32).astype(jnp.bfloat16),
        "tp",
        scatter_dimension=0,
        tiled=True,
    ).astype(jnp.float32)
    summed = mixed.astype(jnp.float32) + 0.5 * down_sum
    scaled = summed * lax.rsqrt(jnp.mean(summed * summed, axis=-1, keepdims=True) + 1e-06)
    return scaled.astype(jnp.bfloat16)


MESH = pl.DeviceIdType.MESH
PIECES = 2


def layer_kernel(
    n, tp, chunk,
    q_ref, k_ref, v_ref, gt_ref, residual_ref, w_out_ref, gain_ref, wg_ref, wu_ref, wd_ref,
    out_ref,
    k_all, v_all, gt_all, att, proj, pc_buf, px_send, px_buf, mixed, normed,
    wg_all, wu_all, wd_all, hid, part, c_buf, x_send, x_buf, z_send, z_buf, total_ref,
    kv_sems, w_sems, y_sems, pc_sems, px_sems, nz_sems, nx_sems, nc_sems, c_sems, x_sems, z_sems, o_sems,
):
    me = lax.axis_index("sp")
    t = lax.axis_index("tp")
    g = lax.axis_index("grp")
    x, c = t // 2, t % 2
    nx = tp // 2
    mate = x * 2 + (1 - c)
    rows = q_ref.shape[0]
    sub = rows // tp
    width = residual_ref.shape[1]
    heads = gt_ref.shape[0]
    head = q_ref.shape[1] // heads
    depth = wg_ref.shape[0]
    ff = wg_ref.shape[1]
    half = depth // 2
    dcols = wd_ref.shape[1]
    dhalf = dcols // 2
    GATE, UP, DOWN = range(3)

    def across(dx):
        return lax.rem(x + dx, nx)

    def per_me(work):
        for s in range(n):
            pl.when(me == s)(functools.partial(work, s))

    def remote(src, dst, send_sem, recv_sem, target):
        return pltpu.make_async_remote_copy(
            src_ref=src, dst_ref=dst, send_sem=send_sem, recv_sem=recv_sem,
            device_id=target, device_id_type=MESH,
        )

    def arrived(slot, sems, *index):
        remote(slot, slot, sems.at[(0, *index)], sems.at[(1, *index)], {"tp": mate}).wait_recv()

    barrier = pltpu.get_barrier_semaphore()
    for d in range(1, n):
        pl.semaphore_signal(barrier, inc=1, device_id={"sp": lax.rem(me + d, n)}, device_id_type=MESH)
    for dx in range(1, nx):
        pl.semaphore_signal(
            barrier, inc=1, device_id={"tp": across(dx) * 2 + c}, device_id_type=MESH
        )
    pl.semaphore_signal(barrier, inc=1, device_id={"tp": mate}, device_id_type=MESH)
    pl.semaphore_signal(barrier, inc=1, device_id={"grp": 1 - g}, device_id_type=MESH)
    pl.semaphore_wait(barrier, n - 1 + nx - 1 + 2)

    sent = [[] for _ in range(n)]

    def launch(s, make):
        make().start()
        sent[s].append(make)

    def kv_copy(s, o, i):
        own = (k_ref, v_ref, gt_ref)[i]
        held = (k_all, v_all, gt_all)[i].at[min(o, n - 2)]
        return remote(
            own if o == s else held, held, kv_sems.at[0, o, i], kv_sems.at[1, o, i], {"sp": s + 1}
        )

    def kv_send(s, o, i):
        launch(s, lambda: kv_copy(s, o, i))

    def kv_arrived(o, i):
        arrived((k_all, v_all, gt_all)[i].at[o], kv_sems, o, i)

    def size_of(j):
        return min(chunk, ff - j * chunk)

    def weight_slot(s, e, i, side):
        size = size_of(s)
        if i == DOWN:
            return wd_all.at[
                :size, pl.ds(pl.multiple_of(e * dcols + side * dhalf, 128), dhalf)
            ]
        held = (wg_all, wu_all)[i]
        return held.at[pl.ds(pl.multiple_of(e * depth + side * half, 16), half), :size]

    def weight_copy(s, j, i):
        place = pl.ds(j * chunk, size_of(j))
        if i == DOWN:
            src = wd_ref.at[place, pl.ds(pl.multiple_of(g * dhalf, 128), dhalf)]
        else:
            src = (wg_ref, wu_ref)[i].at[pl.ds(pl.multiple_of(g * half, 16), half), place]
        return remote(
            src, weight_slot(j, s, i, g), w_sems.at[0, j, i], w_sems.at[1, s, i], {"sp": j}
        )

    def weights(s, targets, pieces):
        for j in targets:
            for i in pieces:
                launch(s, lambda j=j, i=i: weight_copy(s, j, i))

    def relay_weights(s, e, pieces):
        for i in pieces:
            slot = weight_slot(s, e, i, g)
            arrived(slot, w_sems, e, i)

            def make(i=i):
                place = weight_slot(s, e, i, g)
                return remote(
                    place, place, y_sems.at[0, e, i], y_sems.at[1, e, i], {"grp": 1 - g}
                )

            launch(s, make)

    def weights_there(s, e, pieces):
        for i in pieces:
            arrived(weight_slot(s, e, i, 1 - g), y_sems, e, i)

    def own_copies(s):
        size = size_of(s)
        mine = pl.ds(s * chunk, size)
        return (
            pltpu.make_async_copy(
                wg_ref.at[:, mine], wg_all.at[pl.ds(s * depth, depth), :size], o_sems.at[0]
            ),
            pltpu.make_async_copy(
                wu_ref.at[:, mine], wu_all.at[pl.ds(s * depth, depth), :size], o_sems.at[1]
            ),
            pltpu.make_async_copy(
                wd_ref.at[mine, :], wd_all.at[:size, pl.ds(s * dcols, dcols)], o_sems.at[2]
            ),
        )

    def opening(s):
        if s < n - 1:
            for i in range(3):
                kv_send(s, s, i)
        weights(s, range(s - 1, -1, -1), (GATE, UP))
        if s == 0:
            weights(s, [1], (GATE, UP))
        for copy in own_copies(s):
            copy.start()
        size = size_of(s)
        if size < chunk:
            wg_all[:, size:] = jnp.zeros((n * depth, chunk - size), jnp.bfloat16)
            wu_all[:, size:] = jnp.zeros((n * depth, chunk - size), jnp.bfloat16)
            wd_all[size:, :] = jnp.zeros((chunk - size, n * dcols), jnp.bfloat16)
        for o in range(s, n - 1):
            k_all[o] = jnp.zeros_like(k_ref)
            v_all[o] = jnp.zeros_like(v_ref)
            gt_all[o] = jnp.zeros_like(gt_ref)
        for o in range(s - 1, -1, -1):
            for i in range(3):
                kv_arrived(o, i)
                if s < n - 1:
                    kv_send(s, o, i)
        if 0 < s < n - 1:
            weights(s, [s + 1], (GATE, UP))

    per_me(opening)

    pair = 128 // head
    lane = lax.broadcasted_iota(jnp.int32, (rows, 128), 1)
    causal = lax.broadcasted_iota(jnp.int32, (rows, rows), 0) >= lax.broadcasted_iota(
        jnp.int32, (rows, rows), 1
    )
    contract = (((1,), (1,)), ((), ()))
    filler = -heads % 8
    gates = gt_ref[...]
    if filler:
        gates = jnp.concatenate([gates, jnp.zeros((filler, rows), jnp.float32)], axis=0)
    gates = gates.T
    for p in range(heads // pair):
        cols = slice(p * 128, (p + 1) * 128)
        q_pair = q_ref[:, cols]
        joined = jnp.zeros((rows, 128), jnp.float32)
        for i in range(pair):
            h = p * pair + i
            inside = (lane >= i * head) & (lane < (i + 1) * head)
            q_head = jnp.where(inside, q_pair, jnp.zeros_like(q_pair))
            g_query = gates[:, h : h + 1]
            scores = []
            for o in range(n):
                k_pair = k_ref[:, cols] if o == n - 1 else k_all[o, :, cols]
                g_key = gt_ref[h : h + 1, :] if o == n - 1 else gt_all[o, h : h + 1, :]
                score = (
                    lax.dot_general(q_head, k_pair, contract, preferred_element_type=jnp.float32)
                    * head ** (-0.5)
                    + g_query
                    - g_key
                )
                allowed = causal if o == n - 1 else (jnp.zeros((rows, rows), jnp.int32) + me) > o
                scores.append(jnp.where(allowed, score, -1e30))
            peak = functools.reduce(
                jnp.maximum, [jnp.max(score, axis=-1, keepdims=True) for score in scores]
            )
            total = jnp.zeros((rows, 1), jnp.float32)
            summed = jnp.zeros((rows, 128), jnp.float32)
            for o in range(n):
                v_pair = v_ref[:, cols] if o == n - 1 else v_all[o, :, cols]
                weight = jnp.exp(scores[o] - peak)
                total += jnp.sum(weight, axis=-1, keepdims=True)
                summed += jnp.dot(
                    weight.astype(jnp.bfloat16), v_pair, preferred_element_type=jnp.float32
                )
            joined = jnp.where(inside, summed / total, joined)
        att[:, cols] = joined.astype(jnp.bfloat16)

    for k in range(width // 512):
        cols = slice(k * 512, (k + 1) * 512)
        proj[:, cols] = jnp.dot(
            att[...], w_out_ref[:, cols], preferred_element_type=jnp.float32
        ).astype(jnp.bfloat16)

    def block(index):
        return pl.ds(pl.multiple_of(index * sub, sub), sub)

    pc = [
        remote(
            proj.at[block(across(dx) * 2 + 1 - c)], pc_buf.at[dx],
            pc_sems.at[0, dx], pc_sems.at[1, dx], {"tp": mate},
        )
        for dx in range(nx)
    ]
    for dx in (*range(1, nx), 0):
        pc[dx].start()
    px = [
        remote(
            px_send.at[dx], px_buf.at[dx], px_sems.at[0, dx], px_sems.at[1, dx],
            {"tp": across(dx) * 2 + c},
        )
        for dx in range(nx)
    ]
    for dx in range(1, nx):
        pc[dx].wait_recv()
        px_send[dx] = (
            proj[block(across(dx) * 2 + c), :].astype(jnp.float32) + pc_buf[dx].astype(jnp.float32)
        ).astype(jnp.bfloat16)
        px[dx].start()
    pc[0].wait_recv()
    acc = proj[block(t), :].astype(jnp.float32) + pc_buf[0].astype(jnp.float32)
    for dx in range(1, nx):
        px[dx].wait_recv()
        acc += px_buf[dx].astype(jnp.float32)
    mix = (residual_ref[block(t), :].astype(jnp.float32) + acc).astype(jnp.bfloat16)
    mixed[...] = mix
    floats = mix.astype(jnp.float32)
    scale = lax.rsqrt(jnp.mean(floats * floats, axis=-1, keepdims=True) + 1e-06)
    normed[me, t] = (floats * scale * gain_ref[...]).astype(jnp.bfloat16)

    span = width // PIECES

    def row_slot(o, owner, k):
        return normed.at[o, owner, :, k * span : (k + 1) * span]

    def pass_rows(s, o, k):
        for way, j in ((0, s + 1), (1, s - 1)):
            if 0 <= j < n and (o == s or (o < s) == (way == 0)):

                def make(way=way, j=j):
                    slot = row_slot(o, t, k)
                    return remote(
                        slot, slot, nz_sems.at[way, o, k], nz_sems.at[2, o, k], {"sp": j}
                    )

                launch(s, make)

    def spread_rows(s, o, k):
        def to_mate():
            slot = row_slot(o, t, k)
            return remote(slot, slot, nc_sems.at[0, o, 0, k], nc_sems.at[1, o, 0, k], {"tp": mate})

        for dx in range(1, nx):

            def over(dx=dx):
                slot = row_slot(o, t, k)
                return remote(
                    slot, slot, nx_sems.at[0, o, dx, k], nx_sems.at[1, o, dx, k],
                    {"tp": across(dx) * 2 + c},
                )

            launch(s, over)
        launch(s, to_mate)

    def rows_in(s, *origins):
        for o in origins:
            for k in range(PIECES):
                slot = row_slot(o, t, k)
                remote(
                    slot, slot, nz_sems.at[0, o, k], nz_sems.at[2, o, k], {"tp": mate}
                ).wait_recv()
                pass_rows(s, o, k)
                spread_rows(s, o, k)

    def hand_over(s, *origins):
        for o in origins:
            for k in range(PIECES):
                for dx in range(1, nx):
                    owner = lax.rem(x + nx - dx, nx) * 2 + c
                    arrived(row_slot(o, owner, k), nx_sems, o, dx, k)

                    def make(o=o, dx=dx, k=k):
                        slot = row_slot(o, lax.rem(x + nx - dx, nx) * 2 + c, k)
                        return remote(
                            slot, slot, nc_sems.at[0, o, dx, k], nc_sems.at[1, o, dx, k],
                            {"tp": mate},
                        )

                    launch(s, make)

    def rows_ready(o):
        for k in range(PIECES):
            for dx in range(nx):
                owner = lax.rem(x + nx - dx, nx) * 2 + 1 - c
                arrived(row_slot(o, owner, k), nc_sems, o, dx, k)

    def exchange(s):
        up, down = range(s + 1, n), range(s - 1, -1, -1)
        below, above = list(down), list(up)
        for k in range(PIECES):
            pass_rows(s, s, k)
            spread_rows(s, s, k)
        if s == 0:
            weights(s, range(2, n), (GATE, UP))
        if s == 0:
            weights(s, up, (DOWN,))
        if s == n - 1:
            weights(s, down, (DOWN,))
        if 0 < s < n - 1:
            if s == 1:
                weights(s, [0], (DOWN,))
            if s == n - 2:
                weights(s, [n - 1], (DOWN,))
        first, second = (below, above) if s >= n // 2 else (above, below)
        near = second + first if 0 < s < n - 1 else first
        if 0 < s < n - 1:
            relay_weights(s, first[0], (GATE, UP))
        hand_over(s, s)
        if s == 0 or s == n - 1:
            relay_weights(s, near[0], (GATE, UP))
            for k, o in enumerate(near):
                rows_in(s, o)
                if k:
                    relay_weights(s, o, (GATE, UP))
                    hand_over(s, near[k - 1])
            hand_over(s, near[-1])
        else:
            rows_in(s, *below)
            if s < n - 2:
                weights(s, range(s + 2, n), (GATE, UP))
                weights(s, range(s + 1, n), (DOWN,))
            hand_over(s, *below)
            rest = [e for e in below + above if e != first[0]]
            for e in rest[:1]:
                relay_weights(s, e, (GATE, UP))
            rows_in(s, *above)
            if s > 1:
                weights(s, down, (DOWN,))
            for e in rest[1:]:
                relay_weights(s, e, (GATE, UP))
            hand_over(s, *above)
        for e in near:
            weights_there(s, e, (GATE, UP))
        for o in range(n):
            rows_ready(o)
        for copy in own_copies(s):
            copy.wait()

    per_me(exchange)

    for j in range(n):
        piece = normed[j].reshape(rows, width)
        gate = jnp.dot(piece, wg_all[...], preferred_element_type=jnp.float32)
        up = jnp.dot(piece, wu_all[...], preferred_element_type=jnp.float32)
        hid[j] = (gate / (1.0 + jnp.exp(-gate)) * up).astype(jnp.bfloat16)

    def span_of(e):
        return slice(e * dcols, (e + 1) * dcols)

    def down_part(e):
        for j in range(n):
            product = jnp.dot(
                hid[j], wd_all[:, span_of(e)], preferred_element_type=jnp.float32
            ).astype(jnp.bfloat16)
            part[j, :, :, :, span_of(e)] = product.reshape(nx, 2, sub, dcols)

    def c_copy(j, e):
        return remote(
            part.at[j, :, 1 - c, :, span_of(e)], c_buf.at[j, :, :, span_of(e)],
            c_sems.at[0, j, e], c_sems.at[1, j, e], {"tp": mate},
        )

    def x_copy(j, dx, e):
        return remote(
            x_send.at[j, dx, :, span_of(e)], x_buf.at[j, dx, :, span_of(e)],
            x_sems.at[0, j, dx, e], x_sems.at[1, j, dx, e], {"tp": across(dx) * 2 + c},
        )

    turn = [lax.rem(me + 1 + k, n) for k in range(n)]

    def over_x(e):
        for j in turn:
            c_copy(j, e).start()
        for j in turn:
            c_copy(j, e).wait_recv()
            for dx in range(1, nx):
                x_send[j, dx, :, span_of(e)] = (
                    part[j, across(dx), c, :, span_of(e)].astype(jnp.float32)
                    + c_buf[j, across(dx), :, span_of(e)].astype(jnp.float32)
                ).astype(jnp.bfloat16)
                x_copy(j, dx, e).start()

    def local_sum(j, e):
        acc = part[j, x, c, :, span_of(e)].astype(jnp.float32) + c_buf[
            j, x, :, span_of(e)
        ].astype(jnp.float32)
        for dx in range(1, nx):
            x_copy(j, dx, e).wait_recv()
            acc += x_buf[j, dx, :, span_of(e)].astype(jnp.float32)
        return acc

    def z_in(slot, e):
        place = z_buf.at[slot, :, span_of(e)]
        remote(
            place, place, z_sems.at[0, slot, e], z_sems.at[1, slot, e], {"tp": mate}
        ).wait_recv()
        return z_buf[slot, :, span_of(e)].astype(jnp.float32)

    def over_z(s, e):
        ups = list(range(n - 1, s, -1))
        downs = list(range(s))
        order = ups + downs if s < n // 2 else downs + ups
        for j in order:
            acc = local_sum(j, e)
            to = s + 1 if j > s else s - 1
            behind = s - 1 if j > s else s + 1
            if 0 <= behind < n:
                acc += z_in(j, e)
            z_send[j, :, span_of(e)] = acc.astype(jnp.bfloat16)
            slot = n if to == j and j < s else j

            def make(j=j, slot=slot, to=to):
                return remote(
                    z_send.at[j, :, span_of(e)], z_buf.at[slot, :, span_of(e)],
                    z_sems.at[0, j, e], z_sems.at[1, slot, e], {"sp": to},
                )

            launch(s, make)

    def finish(s, e):
        acc = local_sum(s, e)
        if s > 0:
            acc += z_in(s, e)
        if s < n - 1:
            acc += z_in(n, e)
        total_ref[:, span_of(e)] = mixed[:, span_of(e)].astype(jnp.float32) + 0.5 * acc

    def down_arrived(s, *blocks):
        for e in blocks:
            if e != s:
                relay_weights(s, e, (DOWN,))
        for e in blocks:
            if e != s:
                weights_there(s, e, (DOWN,))

    middle = list(range(1, n - 1))
    ends = [0, n - 1] if n > 1 else [0]
    per_me(lambda s: down_arrived(s, *middle))
    for e in middle:
        down_part(e)
        over_x(e)
    per_me(lambda s: down_arrived(s, *ends))
    for e in ends:
        down_part(e)
        over_x(e)
    for e in middle + ends:
        per_me(lambda s, e=e: over_z(s, e))
        per_me(lambda s, e=e: finish(s, e))
    summed = total_ref[...]
    scale = lax.rsqrt(jnp.mean(summed * summed, axis=-1, keepdims=True) + 1e-06)
    out_ref[...] = (summed * scale).astype(jnp.bfloat16)

    for copy in pc:
        copy.wait_send()
    for dx in range(1, nx):
        px[dx].wait_send()
    for e in range(n):
        for j in range(n):
            c_copy(j, e).wait_send()
            for dx in range(1, nx):
                x_copy(j, dx, e).wait_send()

    def all_sent(s):
        for make in sent[s]:
            make().wait_send()

    per_me(all_sent)


def fused_body(residual, queries, keys, values, log_gates, w_out, norm_gain, w_gate, w_up, w_down):
    n, tp = lax.axis_size("sp"), lax.axis_size("tp")
    rows, width = residual.shape
    sub = rows // tp
    nx = tp // 2
    depth, ff = w_gate.shape
    dcols = w_down.shape[1]
    chunk = window(ff, n)
    gates_t = log_gates.T
    bf16, f32 = jnp.bfloat16, jnp.float32
    shapes = [
        ((n - 1, *keys.shape), bf16),
        ((n - 1, *values.shape), bf16),
        ((n - 1, *gates_t.shape), f32),
        (queries.shape, bf16),
        ((rows, width), bf16),
        ((nx, sub, width), bf16),
        ((nx, sub, width), bf16),
        ((nx, sub, width), bf16),
        ((sub, width), bf16),
        ((n, tp, sub, width), bf16),
        ((n * depth, chunk), bf16),
        ((n * depth, chunk), bf16),
        ((chunk, n * dcols), bf16),
        ((n, rows, chunk), bf16),
        ((n, nx, 2, sub, width), bf16),
        ((n, nx, sub, width), bf16),
        ((n, nx, sub, width), bf16),
        ((n, nx, sub, width), bf16),
        ((n, sub, width), bf16),
        ((n + 1, sub, width), bf16),
        ((sub, width), f32),
    ]
    sems = [
        (2, n, 3),
        (2, n, 3),
        (2, n, 3),
        (2, nx),
        (2, nx),
        (3, n, PIECES),
        (2, n, nx, PIECES),
        (2, n, nx, PIECES),
        (2, n, n),
        (2, n, nx, n),
        (2, n + 1, n),
        (3,),
    ]
    return pl.pallas_call(
        functools.partial(layer_kernel, n, tp, chunk),
        out_shape=jax.ShapeDtypeStruct((sub, width), bf16),
        in_specs=[pl.BlockSpec(memory_space=pltpu.VMEM)] * 7
        + [pl.BlockSpec(memory_space=pl.ANY)] * 3,
        out_specs=pl.BlockSpec(memory_space=pltpu.VMEM),
        scratch_shapes=[pltpu.VMEM(shape, dtype) for shape, dtype in shapes]
        + [pltpu.SemaphoreType.DMA(shape) for shape in sems],
        compiler_params=pltpu.CompilerParams(
            collective_id=0, has_side_effects=True, vmem_limit_bytes=60 * 1024 * 1024
        ),
    )(
        queries, keys, values, gates_t, residual, w_out, norm_gain[None, :],
        w_gate, w_up, w_down,
    )


def window(ff, n):
    return -(-ff // (n * 128)) * 128


def fits(mesh, shapes):
    residual, queries, gates, gate = shapes
    n, tp, grp = mesh.shape["sp"], mesh.shape["tp"], mesh.shape["grp"]
    ff = gate[1] // tp
    heads = gates[1] // tp
    head = queries[1] // gates[1]
    rows = residual[0] // (grp * n)
    return (
        grp == 2
        and 2 <= n <= 4
        and tp % 2 == 0
        and ff % 128 == 0
        and window(ff, n) * (n - 1) < ff
        and 128 % head == 0
        and (heads * head) % 128 == 0
        and rows % (16 * tp) == 0
        and rows * n * residual[1] <= 1 << 21
    )


def solution(mesh):
    in_specs = (
        P(("grp", "sp"), None),
        P(("grp", "sp"), "tp"),
        P(("grp", "sp"), "tp"),
        P(("grp", "sp"), "tp"),
        P(("grp", "sp"), "tp"),
        P("tp", None),
        P(),
        P("sp", "tp"),
        P("sp", "tp"),
        P("tp", "sp"),
    )
    out_specs = P(("grp", "sp", "tp"), None)

    def layer(*args):
        residual, queries, _, _, log_gates, _, _, w_gate, _, _ = args
        shapes = (residual.shape, queries.shape, log_gates.shape, w_gate.shape)
        chosen = fused_body if fits(mesh, shapes) else body
        return jax.shard_map(
            chosen, mesh=mesh, in_specs=in_specs, out_specs=out_specs, check_vma=False
        )(*args)

    return layer
```

time: 146 us -> 162 us (1.11); the launches traced: 145 us -> 162 us
  Pallas kernels: 140 us -> 161 us
  local copies, waits for them, and re-layouts: 4.43 us -> 1.67 us
    pallas_call x1, Pallas kernels: 140 us -> 161 us  [fused_body(): pl.pallas_call(functools.partial(layer_kernel, n, tp, chunk), out_shape=j...]
where the time goes in v1:
time: 162 us
  Pallas kernels  161 us (99%)
  local copies, waits for them, and re-layouts  1.67 us (1%)
    pallas_call x1, Pallas kernels, fused_body(): pl.pallas_call(functools.partial(layer_kernel, n, tp, chunk), out_shape=j...  161 us

profile of v1, /device:TPU:0, one launch (start us, length us, event | category | flops | bytes accessed | tf_op | source)
XLA Modules:
  0.0 162.3 jit_solution(8709563888009586338)
XLA Ops:
  0.0 160.6 %shard_map.100 = bf16[64,2048]{1,0:T(8,128)(2,1)} custom-call(bf16[256,256]{1,0:T(8,128)(2,1)} %q_ref.1, bf16[256,256]{1,0:T(8,128)(2,1)} %k_ref.1, bf16[256,256]{1,0:T(8,128)(2,1)} %v_ref.1, f32[4,256]{1,0:T(4,128)} %bitcast.3, bf16[256,2048]{1,0:T(8,128)(2,1)} %residual_ref.1, bf16[256,2048]{1,0:T(8,128)(2,1)} %w_out_ref.1, f32[1,2048]{1,0:T(1,128)} %bitcast.2, ...), custom_call_target="tpu_custom_call" | custom-call | tf_op jit(solution)/shard_map/pallas_call | solution.py:666
  160.6 1.7 %copy.12 = bf16[64,2048]{1,0:T(8,128)(2,1)} copy(bf16[64,2048]{1,0:T(8,128)(2,1)} %shard_map.100) | data formatting | bytes 524288

commit v2 on v1

--- a/solution.py
+++ b/solution.py
@@ -117,6 +117,50 @@
 
 MESH = pl.DeviceIdType.MESH
 PIECES = 2
+OPENING = (
+    (("kv",), ("gu", 1), ("dn", 1), ("gu", 2, 3), ("prep",)),
+    (("kv",), ("gu", 0), ("dn", 0), ("prep",), ("kv_in", 0), ("gu", 2, 3), ("fwd", 2)),
+    (("kv",), ("gu", 1, 0), ("prep",), ("kv_in", 1), ("kv_in", 0), ("gu", 3), ("dn", 3), ("fwd", 3)),
+    (("gu", 2), ("dn", 2), ("gu", 1, 0), ("prep",), ("kv_in", 2), ("kv_in", 1), ("kv_in", 0)),
+)
+EXCHANGE = (
+    (
+        ("own",), ("fwd", 1), ("hand", 0), ("fwd", 3), ("fwd", 2), ("fwd_dn", 1), ("in", 1),
+        ("in", 2), ("hand", 1), ("in", 3), ("dn", 2, 3), ("hand", 2), ("hand", 3),
+    ),
+    (
+        ("own",), ("fwd", 0), ("fwd", 3), ("hand", 1), ("fwd_dn", 0), ("in", 2), ("in", 0),
+        ("dn", 2, 3), ("in", 3), ("hand", 2), ("hand", 0), ("hand", 3),
+    ),
+    (
+        ("own",), ("fwd", 0), ("hand", 2), ("in", 3), ("dn", 1, 0), ("fwd_dn", 3), ("fwd", 1),
+        ("in", 1), ("hand", 3), ("in", 0), ("hand", 1), ("hand", 0),
+    ),
+    (
+        ("own",), ("fwd", 2), ("fwd", 0), ("hand", 3), ("fwd_dn", 2), ("in", 2), ("fwd", 1),
+        ("in", 1), ("dn", 1, 0), ("hand", 2), ("in", 0), ("hand", 1), ("hand", 0),
+    ),
+)
+ROW_ORDER = ((0, 1, 2, 3), (1, 2, 3, 0), (2, 1, 0, 3), (3, 2, 1, 0))
+COLUMN_ORDER = ((0, 1, 2, 3), (1, 0, 2, 3), (2, 3, 1, 0), (3, 2, 1, 0))
+
+
+def line_tasks(n):
+    ready = {}
+
+    def when(s, j, e):
+        if (s, j, e) not in ready:
+            own = COLUMN_ORDER[s].index(e) * n + (ROW_ORDER[s].index(j) - 1) % n
+            if j == s:
+                before = [(b, j, e) for b in (s - 1, s + 1) if 0 <= b < n]
+            else:
+                b = s - 1 if j > s else s + 1
+                before = [(b, j, e)] if 0 <= b < n else []
+            ready[s, j, e] = max([own] + [when(*task) + 2 for task in before])
+        return ready[s, j, e]
+
+    every = [(j, e) for j in range(n) for e in range(n)]
+    return [sorted(every, key=lambda task: (task[0] == s, when(s, *task), task)) for s in range(n)]
 
 
 def layer_kernel(
@@ -150,7 +194,10 @@
 
     def per_me(work):
         for s in range(n):
-            pl.when(me == s)(functools.partial(work, s))
+
+            @pl.when(me == s)
+            def _(s=s):
+                work(s)
 
     def remote(src, dst, send_sem, recv_sem, target):
         return pltpu.make_async_remote_copy(
@@ -250,13 +297,84 @@
             ),
         )
 
-    def opening(s):
+    span = width // PIECES
+
+    def row_slot(o, owner, k):
+        return normed.at[o, owner, :, k * span : (k + 1) * span]
+
+    def pass_rows(s, o, k):
+        for way, j in ((0, s + 1), (1, s - 1)):
+            if 0 <= j < n and (o == s or (o < s) == (way == 0)):
+
+                def make(way=way, j=j):
+                    slot = row_slot(o, t, k)
+                    return remote(
+                        slot, slot, nz_sems.at[way, o, k], nz_sems.at[2, o, k], {"sp": j}
+                    )
+
+                launch(s, make)
+
+    def spread_rows(s, o, k):
+        def to_mate():
+            slot = row_slot(o, t, k)
+            return remote(slot, slot, nc_sems.at[0, o, 0, k], nc_sems.at[1, o, 0, k], {"tp": mate})
+
+        for dx in range(1, nx):
+
+            def over(dx=dx):
+                slot = row_slot(o, t, k)
+                return remote(
+                    slot, slot, nx_sems.at[0, o, dx, k], nx_sems.at[1, o, dx, k],
+                    {"tp": across(dx) * 2 + c},
+                )
+
+            launch(s, over)
+        launch(s, to_mate)
+
+    def rows_in(s, *origins):
+        for o in origins:
+            for k in range(PIECES):
+                slot = row_slot(o, t, k)
+                remote(
+                    slot, slot, nz_sems.at[0, o, k], nz_sems.at[2, o, k], {"tp": mate}
+                ).wait_recv()
+                pass_rows(s, o, k)
+                spread_rows(s, o, k)
+
+    def hand_over(s, *origins):
+        for o in origins:
+            for k in range(PIECES):
+                for dx in range(1, nx):
+                    owner = lax.rem(x + nx - dx, nx) * 2 + c
+                    arrived(row_slot(o, owner, k), nx_sems, o, dx, k)
+
+                    def make(o=o, dx=dx, k=k):
+                        slot = row_slot(o, lax.rem(x + nx - dx, nx) * 2 + c, k)
+                        return remote(
+                            slot, slot, nc_sems.at[0, o, dx, k], nc_sems.at[1, o, dx, k],
+                            {"tp": mate},
+                        )
+
+                    launch(s, make)
+
+    def rows_ready(o):
+        for k in range(PIECES):
+            for dx in range(nx):
+                owner = lax.rem(x + nx - dx, nx) * 2 + 1 - c
+                arrived(row_slot(o, owner, k), nc_sems, o, dx, k)
+
+    def kv_in(s, o):
+        for i in range(3):
+            kv_arrived(o, i)
+            if s < n - 1:
+                kv_send(s, o, i)
+
+    def kv_out(s):
         if s < n - 1:
             for i in range(3):
                 kv_send(s, s, i)
-        weights(s, range(s - 1, -1, -1), (GATE, UP))
-        if s == 0:
-            weights(s, [1], (GATE, UP))
+
+    def prepare(s):
         for copy in own_copies(s):
             copy.start()
         size = size_of(s)
@@ -268,15 +386,30 @@
             k_all[o] = jnp.zeros_like(k_ref)
             v_all[o] = jnp.zeros_like(v_ref)
             gt_all[o] = jnp.zeros_like(gt_ref)
-        for o in range(s - 1, -1, -1):
-            for i in range(3):
-                kv_arrived(o, i)
-                if s < n - 1:
-                    kv_send(s, o, i)
-        if 0 < s < n - 1:
-            weights(s, [s + 1], (GATE, UP))
-
-    per_me(opening)
+
+    def own_rows(s):
+        for k in range(PIECES):
+            pass_rows(s, s, k)
+            spread_rows(s, s, k)
+
+    steps = {
+        "kv": kv_out,
+        "kv_in": kv_in,
+        "own": own_rows,
+        "gu": lambda s, *to: weights(s, to, (GATE, UP)),
+        "dn": lambda s, *to: weights(s, to, (DOWN,)),
+        "in": lambda s, *origins: rows_in(s, *origins),
+        "hand": lambda s, *origins: hand_over(s, *origins),
+        "fwd": lambda s, e: relay_weights(s, e, (GATE, UP)),
+        "fwd_dn": lambda s, e: relay_weights(s, e, (DOWN,)),
+        "prep": prepare,
+    }
+
+    def follow(s, plan):
+        for name, *where in plan:
+            steps[name](s, *where)
+
+    per_me(lambda s: follow(s, OPENING[s]))
 
     pair = 128 // head
     lane = lax.broadcasted_iota(jnp.int32, (rows, 128), 1)
@@ -367,167 +500,61 @@
     scale = lax.rsqrt(jnp.mean(floats * floats, axis=-1, keepdims=True) + 1e-06)
     normed[me, t] = (floats * scale * gain_ref[...]).astype(jnp.bfloat16)
 
-    span = width // PIECES
-
-    def row_slot(o, owner, k):
-        return normed.at[o, owner, :, k * span : (k + 1) * span]
-
-    def pass_rows(s, o, k):
-        for way, j in ((0, s + 1), (1, s - 1)):
-            if 0 <= j < n and (o == s or (o < s) == (way == 0)):
-
-                def make(way=way, j=j):
-                    slot = row_slot(o, t, k)
-                    return remote(
-                        slot, slot, nz_sems.at[way, o, k], nz_sems.at[2, o, k], {"sp": j}
-                    )
-
-                launch(s, make)
-
-    def spread_rows(s, o, k):
-        def to_mate():
-            slot = row_slot(o, t, k)
-            return remote(slot, slot, nc_sems.at[0, o, 0, k], nc_sems.at[1, o, 0, k], {"tp": mate})
-
-        for dx in range(1, nx):
-
-            def over(dx=dx):
-                slot = row_slot(o, t, k)
-                return remote(
-                    slot, slot, nx_sems.at[0, o, dx, k], nx_sems.at[1, o, dx, k],
-                    {"tp": across(dx) * 2 + c},
-                )
-
-            launch(s, over)
-        launch(s, to_mate)
-
-    def rows_in(s, *origins):
-        for o in origins:
-            for k in range(PIECES):
-                slot = row_slot(o, t, k)
-                remote(
-                    slot, slot, nz_sems.at[0, o, k], nz_sems.at[2, o, k], {"tp": mate}
-                ).wait_recv()
-                pass_rows(s, o, k)
-                spread_rows(s, o, k)
-
-    def hand_over(s, *origins):
-        for o in origins:
-            for k in range(PIECES):
-                for dx in range(1, nx):
-                    owner = lax.rem(x + nx - dx, nx) * 2 + c
-                    arrived(row_slot(o, owner, k), nx_sems, o, dx, k)
-
-                    def make(o=o, dx=dx, k=k):
-                        slot = row_slot(o, lax.rem(x + nx - dx, nx) * 2 + c, k)
-                        return remote(
-                            slot, slot, nc_sems.at[0, o, dx, k], nc_sems.at[1, o, dx, k],
-                            {"tp": mate},
-                        )
-
-                    launch(s, make)
-
-    def rows_ready(o):
-        for k in range(PIECES):
-            for dx in range(nx):
-                owner = lax.rem(x + nx - dx, nx) * 2 + 1 - c
-                arrived(row_slot(o, owner, k), nc_sems, o, dx, k)
-
     def exchange(s):
-        up, down = range(s + 1, n), range(s - 1, -1, -1)
-        below, above = list(down), list(up)
-        for k in range(PIECES):
-            pass_rows(s, s, k)
-            spread_rows(s, s, k)
-        if s == 0:
-            weights(s, range(2, n), (GATE, UP))
-        if s == 0:
-            weights(s, up, (DOWN,))
-        if s == n - 1:
-            weights(s, down, (DOWN,))
-        if 0 < s < n - 1:
-            if s == 1:
-                weights(s, [0], (DOWN,))
-            if s == n - 2:
-                weights(s, [n - 1], (DOWN,))
-        first, second = (below, above) if s >= n // 2 else (above, below)
-        near = second + first if 0 < s < n - 1 else first
-        if 0 < s < n - 1:
-            relay_weights(s, first[0], (GATE, UP))
-        hand_over(s, s)
-        if s == 0 or s == n - 1:
-            relay_weights(s, near[0], (GATE, UP))
-            for k, o in enumerate(near):
-                rows_in(s, o)
-                if k:
-                    relay_weights(s, o, (GATE, UP))
-                    hand_over(s, near[k - 1])
-            hand_over(s, near[-1])
-        else:
-            rows_in(s, *below)
-            if s < n - 2:
-                weights(s, range(s + 2, n), (GATE, UP))
-                weights(s, range(s + 1, n), (DOWN,))
-            hand_over(s, *below)
-            rest = [e for e in below + above if e != first[0]]
-            for e in rest[:1]:
-                relay_weights(s, e, (GATE, UP))
-            rows_in(s, *above)
-            if s > 1:
-                weights(s, down, (DOWN,))
-            for e in rest[1:]:
-                relay_weights(s, e, (GATE, UP))
-            hand_over(s, *above)
-        for e in near:
-            weights_there(s, e, (GATE, UP))
-        for o in range(n):
-            rows_ready(o)
+        follow(s, EXCHANGE[s])
+        for e in range(n):
+            if e != s:
+                weights_there(s, e, (GATE, UP))
         for copy in own_copies(s):
             copy.wait()
 
     per_me(exchange)
 
-    for j in range(n):
+    def span_of(e):
+        return pl.ds(e * dcols if isinstance(e, int) else pl.multiple_of(e * dcols, 128), dcols)
+
+    def c_copy(j, e):
+        return remote(
+            part.at[j, :, 1 - c, :, span_of(e)], c_buf.at[j, :, :, span_of(e)],
+            c_sems.at[0, j, e], c_sems.at[1, j, e], {"tp": mate},
+        )
+
+    def x_copy(j, dx, e):
+        return remote(
+            x_send.at[j, dx, :, span_of(e)], x_buf.at[j, dx, :, span_of(e)],
+            x_sems.at[0, j, dx, e], x_sems.at[1, j, dx, e], {"tp": across(dx) * 2 + c},
+        )
+
+    high = me // (n // 2)
+    row_order = [lax.rem(me + n + k * (1 - 2 * high), n) for k in range(n)]
+    column_order = [me, me + 1 - 2 * lax.rem(me, 2), n // 2 - high, (n - 1) * (1 - high)]
+
+    def down_part(j, e):
+        product = jnp.dot(
+            hid[j], wd_all[:, span_of(e)], preferred_element_type=jnp.float32
+        ).astype(jnp.bfloat16)
+        part[j, :, :, :, span_of(e)] = product.reshape(nx, 2, sub, dcols)
+        c_copy(j, e).start()
+
+    def over_x(j, e):
+        c_copy(j, e).wait_recv()
+        for dx in range(1, nx):
+            x_send[j, dx, :, span_of(e)] = (
+                part[j, across(dx), c, :, span_of(e)].astype(jnp.float32)
+                + c_buf[j, across(dx), :, span_of(e)].astype(jnp.float32)
+            ).astype(jnp.bfloat16)
+            x_copy(j, dx, e).start()
+
+    for k, j in enumerate(row_order):
+        per_me(lambda s: rows_ready(ROW_ORDER[s][k]))
         piece = normed[j].reshape(rows, width)
         gate = jnp.dot(piece, wg_all[...], preferred_element_type=jnp.float32)
         up = jnp.dot(piece, wu_all[...], preferred_element_type=jnp.float32)
         hid[j] = (gate / (1.0 + jnp.exp(-gate)) * up).astype(jnp.bfloat16)
-
-    def span_of(e):
-        return slice(e * dcols, (e + 1) * dcols)
-
-    def down_part(e):
-        for j in range(n):
-            product = jnp.dot(
-                hid[j], wd_all[:, span_of(e)], preferred_element_type=jnp.float32
-            ).astype(jnp.bfloat16)
-            part[j, :, :, :, span_of(e)] = product.reshape(nx, 2, sub, dcols)
-
-    def c_copy(j, e):
-        return remote(
-            part.at[j, :, 1 - c, :, span_of(e)], c_buf.at[j, :, :, span_of(e)],
-            c_sems.at[0, j, e], c_sems.at[1, j, e], {"tp": mate},
-        )
-
-    def x_copy(j, dx, e):
-        return remote(
-            x_send.at[j, dx, :, span_of(e)], x_buf.at[j, dx, :, span_of(e)],
-            x_sems.at[0, j, dx, e], x_sems.at[1, j, dx, e], {"tp": across(dx) * 2 + c},
-        )
-
-    turn = [lax.rem(me + 1 + k, n) for k in range(n)]
-
-    def over_x(e):
-        for j in turn:
-            c_copy(j, e).start()
-        for j in turn:
-            c_copy(j, e).wait_recv()
-            for dx in range(1, nx):
-                x_send[j, dx, :, span_of(e)] = (
-                    part[j, across(dx), c, :, span_of(e)].astype(jnp.float32)
-                    + c_buf[j, across(dx), :, span_of(e)].astype(jnp.float32)
-                ).astype(jnp.bfloat16)
-                x_copy(j, dx, e).start()
+        down_part(j, column_order[0])
+        if k:
+            over_x(row_order[k - 1], column_order[0])
+    over_x(row_order[-1], column_order[0])
 
     def local_sum(j, e):
         acc = part[j, x, c, :, span_of(e)].astype(jnp.float32) + c_buf[
@@ -545,26 +572,22 @@
         ).wait_recv()
         return z_buf[slot, :, span_of(e)].astype(jnp.float32)
 
-    def over_z(s, e):
-        ups = list(range(n - 1, s, -1))
-        downs = list(range(s))
-        order = ups + downs if s < n // 2 else downs + ups
-        for j in order:
-            acc = local_sum(j, e)
-            to = s + 1 if j > s else s - 1
-            behind = s - 1 if j > s else s + 1
-            if 0 <= behind < n:
-                acc += z_in(j, e)
-            z_send[j, :, span_of(e)] = acc.astype(jnp.bfloat16)
-            slot = n if to == j and j < s else j
-
-            def make(j=j, slot=slot, to=to):
-                return remote(
-                    z_send.at[j, :, span_of(e)], z_buf.at[slot, :, span_of(e)],
-                    z_sems.at[0, j, e], z_sems.at[1, slot, e], {"sp": to},
-                )
-
-            launch(s, make)
+    def over_z(s, j, e):
+        acc = local_sum(j, e)
+        to = s + 1 if j > s else s - 1
+        behind = s - 1 if j > s else s + 1
+        if 0 <= behind < n:
+            acc += z_in(j, e)
+        z_send[j, :, span_of(e)] = acc.astype(jnp.bfloat16)
+        slot = n if to == j and j < s else j
+
+        def make():
+            return remote(
+                z_send.at[j, :, span_of(e)], z_buf.at[slot, :, span_of(e)],
+                z_sems.at[0, j, e], z_sems.at[1, slot, e], {"sp": to},
+            )
+
+        launch(s, make)
 
     def finish(s, e):
         acc = local_sum(s, e)
@@ -574,27 +597,38 @@
             acc += z_in(n, e)
         total_ref[:, span_of(e)] = mixed[:, span_of(e)].astype(jnp.float32) + 0.5 * acc
 
-    def down_arrived(s, *blocks):
-        for e in blocks:
-            if e != s:
-                relay_weights(s, e, (DOWN,))
-        for e in blocks:
-            if e != s:
-                weights_there(s, e, (DOWN,))
-
-    middle = list(range(1, n - 1))
-    ends = [0, n - 1] if n > 1 else [0]
-    per_me(lambda s: down_arrived(s, *middle))
-    for e in middle:
-        down_part(e)
-        over_x(e)
-    per_me(lambda s: down_arrived(s, *ends))
-    for e in ends:
-        down_part(e)
-        over_x(e)
-    for e in middle + ends:
-        per_me(lambda s, e=e: over_z(s, e))
-        per_me(lambda s, e=e: finish(s, e))
+    def down_arrived(s, e):
+        if (("fwd_dn", e)) not in EXCHANGE[s]:
+            relay_weights(s, e, (DOWN,))
+
+    def down_there(s, e):
+        weights_there(s, e, (DOWN,))
+
+    order = line_tasks(n)
+
+    def early(s, j, e):
+        return s in (0, n - 1) and e == s and j != s
+
+    def along(s, first):
+        for j, e in order[s]:
+            if early(s, j, e) == first:
+                if j == s:
+                    finish(s, e)
+                else:
+                    over_z(s, j, e)
+
+    for q in range(1, n):
+        if q == 1:
+            per_me(lambda s: [down_arrived(s, e) for e in COLUMN_ORDER[s][1:]])
+        per_me(lambda s: down_there(s, COLUMN_ORDER[s][q]))
+        for j in row_order:
+            down_part(j, column_order[q])
+        for j in row_order[1:] + row_order[:1]:
+            over_x(j, column_order[q])
+        if q == 1:
+            per_me(lambda s: along(s, True))
+
+    per_me(lambda s: along(s, False))
     summed = total_ref[...]
     scale = lax.rsqrt(jnp.mean(summed * summed, axis=-1, keepdims=True) + 1e-06)
     out_ref[...] = (summed * scale).astype(jnp.bfloat16)
@@ -693,7 +727,7 @@
     rows = residual[0] // (grp * n)
     return (
         grp == 2
-        and 2 <= n <= 4
+        and n == 4
         and tp % 2 == 0
         and ff % 128 == 0
         and window(ff, n) * (n - 1) < ff

time: 162 us -> 114 us (0.70)
  Pallas kernels: 161 us -> 112 us
    pallas_call x1, Pallas kernels: 161 us -> 112 us  [fused_body(): pl.pallas_call(functools.partial(layer_kernel, n, tp, chunk), out_shape=j...]
where the time goes in v2:
time: 114 us
  Pallas kernels  112 us (98%)
  local copies, waits for them, and re-layouts  1.67 us (1%)
    pallas_call x1, Pallas kernels, fused_body(): pl.pallas_call(functools.partial(layer_kernel, n, tp, chunk), out_shape=j...  112 us

profile of v2, /device:TPU:0, one launch (start us, length us, event | category | flops | bytes accessed | tf_op | source)
XLA Modules:
  0.0 113.9 jit_solution(17162924431093274589)
XLA Ops:
  0.0 112.2 %shard_map.100 = bf16[64,2048]{1,0:T(8,128)(2,1)} custom-call(bf16[256,256]{1,0:T(8,128)(2,1)} %q_ref.1, bf16[256,256]{1,0:T(8,128)(2,1)} %k_ref.1, bf16[256,256]{1,0:T(8,128)(2,1)} %v_ref.1, f32[4,256]{1,0:T(4,128)} %bitcast.3, bf16[256,2048]{1,0:T(8,128)(2,1)} %residual_ref.1, bf16[256,2048]{1,0:T(8,128)(2,1)} %w_out_ref.1, f32[1,2048]{1,0:T(1,128)} %bitcast.2, ...), custom_call_target="tpu_custom_call" | custom-call | tf_op jit(solution)/shard_map/pallas_call | solution.py:700
  112.2 1.7 %copy.12 = bf16[64,2048]{1,0:T(8,128)(2,1)} copy(bf16[64,2048]{1,0:T(8,128)(2,1)} %shard_map.100) | data formatting | bytes 524288

commit v3 on v2

--- a/solution.py
+++ b/solution.py
@@ -126,50 +126,81 @@
 EXCHANGE = (
     (
         ("own",), ("fwd", 1), ("hand", 0), ("fwd", 3), ("fwd", 2), ("fwd_dn", 1), ("in", 1),
-        ("in", 2), ("hand", 1), ("in", 3), ("dn", 2, 3), ("hand", 2), ("hand", 3),
+        ("in", 2), ("hand", 1), ("in", 3), ("dn", 2, 3), ("hand", 2),
     ),
     (
         ("own",), ("fwd", 0), ("fwd", 3), ("hand", 1), ("fwd_dn", 0), ("in", 2), ("in", 0),
-        ("dn", 2, 3), ("in", 3), ("hand", 2), ("hand", 0), ("hand", 3),
+        ("dn", 2, 3), ("in", 3), ("hand", 0), ("hand", 2),
     ),
     (
         ("own",), ("fwd", 0), ("hand", 2), ("in", 3), ("dn", 1, 0), ("fwd_dn", 3), ("fwd", 1),
-        ("in", 1), ("hand", 3), ("in", 0), ("hand", 1), ("hand", 0),
+        ("in", 1), ("hand", 3), ("in", 0), ("hand", 1),
     ),
     (
         ("own",), ("fwd", 2), ("fwd", 0), ("hand", 3), ("fwd_dn", 2), ("in", 2), ("fwd", 1),
-        ("in", 1), ("dn", 1, 0), ("hand", 2), ("in", 0), ("hand", 1), ("hand", 0),
+        ("in", 1), ("dn", 1, 0), ("hand", 2), ("in", 0), ("hand", 1),
     ),
 )
-ROW_ORDER = ((0, 1, 2, 3), (1, 2, 3, 0), (2, 1, 0, 3), (3, 2, 1, 0))
+LAST_ROWS = (3, 3, 0, 0)
+STARTS = (2.0, 9.0, 16.5, 19.5)
+
+
+def stage(n, s, j, e):
+    lower = s < n // 2
+    if j == s or (j > s) != lower or (e < n // 2) != lower:
+        return 2
+    if s in (0, n - 1):
+        return 0 if e == s else 1
+    return 1 if e in (0, n - 1) else 2
+
+
+ROW_ORDER = ((0, 1, 2, 3), (1, 0, 2, 3), (2, 3, 1, 0), (3, 2, 1, 0))
 COLUMN_ORDER = ((0, 1, 2, 3), (1, 0, 2, 3), (2, 3, 1, 0), (3, 2, 1, 0))
 
 
 def line_tasks(n):
-    ready = {}
-
-    def when(s, j, e):
-        if (s, j, e) not in ready:
-            own = COLUMN_ORDER[s].index(e) * n + (ROW_ORDER[s].index(j) - 1) % n
-            if j == s:
-                before = [(b, j, e) for b in (s - 1, s + 1) if 0 <= b < n]
-            else:
-                b = s - 1 if j > s else s + 1
-                before = [(b, j, e)] if 0 <= b < n else []
-            ready[s, j, e] = max([own] + [when(*task) + 2 for task in before])
-        return ready[s, j, e]
-
-    every = [(j, e) for j in range(n) for e in range(n)]
-    return [sorted(every, key=lambda task: (task[0] == s, when(s, *task), task)) for s in range(n)]
+    wire, hop, add = 1.4, 1.8, 0.3
+    base = (STARTS[1] + 2, STARTS[2] + 1, STARTS[3] + 1)
+    term, clock = {}, [0.0] * n
+    for s in range(n):
+        link = 0.0
+        for q, e in enumerate(COLUMN_ORDER[s]):
+            for p in range(n):
+                j = ROW_ORDER[s][p if q == 0 else n - 1 - p]
+                link = max(link, STARTS[q] + (1.6 if q == 0 else 0.2) * p) + wire
+                term[s, j, e] = link + hop
+    waiting = {(s, j, e) for s in range(n) for j in range(n) for e in range(n) if j != s}
+    arrival, links, tasks = {}, {}, [[] for _ in range(n)]
+    while waiting:
+        best = None
+        for s, j, e in waiting:
+            up = j > s
+            behind = s - 1 if up else s + 1
+            if 0 <= behind < n and (s, j, e) not in arrival:
+                continue
+            start = max(term[s, j, e], clock[s], base[stage(n, s, j, e)])
+            start = max(start, arrival.get((s, j, e), 0.0))
+            best = min(best or (start + 1, 0, 0), (start, -abs(j - s), (s, j, e)))
+        start, _, (s, j, e) = best
+        waiting.remove((s, j, e))
+        tasks[s].append((j, e))
+        up = j > s
+        clock[s] = start + add
+        links[s, up] = max(links.get((s, up), 0.0), start + add) + wire
+        arrival[s + 1 if up else s - 1, j, e] = links[s, up] + hop
+    for s in range(n):
+        tasks[s] += [(s, e) for e in COLUMN_ORDER[s]]
+    return tasks
 
 
 def layer_kernel(
     n, tp, chunk,
-    q_ref, k_ref, v_ref, gt_ref, residual_ref, w_out_ref, gain_ref, wg_ref, wu_ref, wd_ref,
+    q_in, k_in, v_in, gt_in, residual_in, w_out_in, gain_in, wg_ref, wu_ref, wd_ref,
     out_ref,
+    q_ref, k_ref, v_ref, gt_ref, residual_ref, w_out_ref, gain_ref,
     k_all, v_all, gt_all, att, proj, pc_buf, px_send, px_buf, mixed, normed,
     wg_all, wu_all, wd_all, hid, part, c_buf, x_send, x_buf, z_send, z_buf, total_ref,
-    kv_sems, w_sems, y_sems, pc_sems, px_sems, nz_sems, nx_sems, nc_sems, c_sems, x_sems, z_sems, o_sems,
+    kv_sems, w_sems, y_sems, pc_sems, px_sems, nz_sems, nx_sems, nc_sems, c_sems, x_sems, z_sems, o_sems, i_sems,
 ):
     me = lax.axis_index("sp")
     t = lax.axis_index("tp")
@@ -217,6 +248,19 @@
         )
     pl.semaphore_signal(barrier, inc=1, device_id={"tp": mate}, device_id_type=MESH)
     pl.semaphore_signal(barrier, inc=1, device_id={"grp": 1 - g}, device_id_type=MESH)
+    staged = [
+        pltpu.make_async_copy(src, dst, i_sems.at[i])
+        for i, (src, dst) in enumerate(
+            (
+                (k_in, k_ref), (v_in, v_ref), (gt_in, gt_ref), (q_in, q_ref),
+                (w_out_in, w_out_ref), (residual_in, residual_ref), (gain_in, gain_ref),
+            )
+        )
+    ]
+    for copy in staged:
+        copy.start()
+    for copy in staged[:3]:
+        copy.wait()
     pl.semaphore_wait(barrier, n - 1 + nx - 1 + 2)
 
     sent = [[] for _ in range(n)]
@@ -411,6 +455,8 @@
 
     per_me(lambda s: follow(s, OPENING[s]))
 
+    for copy in staged[3:]:
+        copy.wait()
     pair = 128 // head
     lane = lax.broadcasted_iota(jnp.int32, (rows, 128), 1)
     causal = lax.broadcasted_iota(jnp.int32, (rows, rows), 0) >= lax.broadcasted_iota(
@@ -526,8 +572,8 @@
         )
 
     high = me // (n // 2)
-    row_order = [lax.rem(me + n + k * (1 - 2 * high), n) for k in range(n)]
-    column_order = [me, me + 1 - 2 * lax.rem(me, 2), n // 2 - high, (n - 1) * (1 - high)]
+    row_order = [me, me + 1 - 2 * lax.rem(me, 2), n // 2 - high, (n - 1) * (1 - high)]
+    column_order = row_order
 
     def down_part(j, e):
         product = jnp.dot(
@@ -545,7 +591,16 @@
             ).astype(jnp.bfloat16)
             x_copy(j, dx, e).start()
 
+    def down_arrived(s, e):
+        if (("fwd_dn", e)) not in EXCHANGE[s]:
+            relay_weights(s, e, (DOWN,))
+
+    def down_there(s, e):
+        weights_there(s, e, (DOWN,))
+
     for k, j in enumerate(row_order):
+        if k == 2:
+            per_me(lambda s: hand_over(s, LAST_ROWS[s]))
         per_me(lambda s: rows_ready(ROW_ORDER[s][k]))
         piece = normed[j].reshape(rows, width)
         gate = jnp.dot(piece, wg_all[...], preferred_element_type=jnp.float32)
@@ -597,21 +652,11 @@
             acc += z_in(n, e)
         total_ref[:, span_of(e)] = mixed[:, span_of(e)].astype(jnp.float32) + 0.5 * acc
 
-    def down_arrived(s, e):
-        if (("fwd_dn", e)) not in EXCHANGE[s]:
-            relay_weights(s, e, (DOWN,))
-
-    def down_there(s, e):
-        weights_there(s, e, (DOWN,))
-
     order = line_tasks(n)
 
-    def early(s, j, e):
-        return s in (0, n - 1) and e == s and j != s
-
-    def along(s, first):
+    def along(s, due):
         for j, e in order[s]:
-            if early(s, j, e) == first:
+            if stage(n, s, j, e) == due:
                 if j == s:
                     finish(s, e)
                 else:
@@ -619,16 +664,18 @@
 
     for q in range(1, n):
         if q == 1:
-            per_me(lambda s: [down_arrived(s, e) for e in COLUMN_ORDER[s][1:]])
+            per_me(lambda s: down_arrived(s, COLUMN_ORDER[s][1]))
         per_me(lambda s: down_there(s, COLUMN_ORDER[s][q]))
-        for j in row_order:
+        for j in row_order[::-1]:
             down_part(j, column_order[q])
-        for j in row_order[1:] + row_order[:1]:
+        for j in row_order[::-1]:
             over_x(j, column_order[q])
         if q == 1:
-            per_me(lambda s: along(s, True))
-
-    per_me(lambda s: along(s, False))
+            per_me(lambda s: [down_arrived(s, e) for e in COLUMN_ORDER[s][2:]])
+        if q < 3:
+            per_me(lambda s: along(s, q - 1))
+
+    per_me(lambda s: along(s, 2))
     summed = total_ref[...]
     scale = lax.rsqrt(jnp.mean(summed * summed, axis=-1, keepdims=True) + 1e-06)
     out_ref[...] = (summed * scale).astype(jnp.bfloat16)
@@ -661,6 +708,13 @@
     gates_t = log_gates.T
     bf16, f32 = jnp.bfloat16, jnp.float32
     shapes = [
+        (queries.shape, bf16),
+        (keys.shape, bf16),
+        (values.shape, bf16),
+        (gates_t.shape, f32),
+        (residual.shape, bf16),
+        (w_out.shape, bf16),
+        ((1, width), f32),
         ((n - 1, *keys.shape), bf16),
         ((n - 1, *values.shape), bf16),
         ((n - 1, *gates_t.shape), f32),
@@ -696,12 +750,12 @@
         (2, n, nx, n),
         (2, n + 1, n),
         (3,),
+        (7,),
     ]
     return pl.pallas_call(
         functools.partial(layer_kernel, n, tp, chunk),
         out_shape=jax.ShapeDtypeStruct((sub, width), bf16),
-        in_specs=[pl.BlockSpec(memory_space=pltpu.VMEM)] * 7
-        + [pl.BlockSpec(memory_space=pl.ANY)] * 3,
+        in_specs=[pl.BlockSpec(memory_space=pl.ANY)] * 10,
         out_specs=pl.BlockSpec(memory_space=pltpu.VMEM),
         scratch_shapes=[pltpu.VMEM(shape, dtype) for shape, dtype in shapes]
         + [pltpu.SemaphoreType.DMA(shape) for shape in sems],

time: 114 us -> 107 us (0.939)
  Pallas kernels: 112 us -> 105 us
    pallas_call x1, Pallas kernels: 112 us -> 105 us  [fused_body(): pl.pallas_call(functools.partial(layer_kernel, n, tp, chunk), out_shape=j...]
where the time goes in v3:
time: 107 us; the launch traced here: 106 us
  Pallas kernels  105 us (98%)
  local copies, waits for them, and re-layouts  1.67 us (2%)
    pallas_call x1, Pallas kernels, fused_body(): pl.pallas_call(functools.partial(layer_kernel, n, tp, chunk), out_shape=j...  105 us

profile of v3, /device:TPU:0, one launch (start us, length us, event | category | flops | bytes accessed | tf_op | source)
XLA Modules:
  0.0 106.5 jit_solution(6865470446313710100)
XLA Ops:
  0.0 104.8 %shard_map.100 = bf16[64,2048]{1,0:T(8,128)(2,1)} custom-call(bf16[256,256]{1,0:T(8,128)(2,1)} %q_in.1, bf16[256,256]{1,0:T(8,128)(2,1)} %k_in.1, bf16[256,256]{1,0:T(8,128)(2,1)} %v_in.1, f32[4,256]{1,0:T(4,128)} %bitcast.3, bf16[256,2048]{1,0:T(8,128)(2,1)} %residual_in.1, bf16[256,2048]{1,0:T(8,128)(2,1)} %w_out_in.1, f32[1,2048]{1,0:T(1,128)} %bitcast.2, ...), custom_call_target="tpu_custom_call" | custom-call | tf_op jit(solution)/shard_map/pallas_call | solution.py:755
  104.8 1.7 %copy.12 = bf16[64,2048]{1,0:T(8,128)(2,1)} copy(bf16[64,2048]{1,0:T(8,128)(2,1)} %shard_map.100) | data formatting | bytes 524288

commit v4 on v3

--- a/solution.py
+++ b/solution.py
@@ -141,8 +141,12 @@
         ("in", 1), ("dn", 1, 0), ("hand", 2), ("in", 0), ("hand", 1),
     ),
 )
-LAST_ROWS = (3, 3, 0, 0)
+LATE = ((("hand", 3),), (("hand", 3),), (("hand", 0),), (("hand", 0),))
 STARTS = (2.0, 9.0, 16.5, 19.5)
+
+
+def direct(n, up, e):
+    return e == (n - 1 if up else 0)
 
 
 def stage(n, s, j, e):
@@ -159,7 +163,7 @@
 
 
 def line_tasks(n):
-    wire, hop, add = 1.4, 1.8, 0.3
+    wire, hop, add = 1.4, 3.5, 0.3
     base = (STARTS[1] + 2, STARTS[2] + 1, STARTS[3] + 1)
     term, clock = {}, [0.0] * n
     for s in range(n):
@@ -176,7 +180,7 @@
         for s, j, e in waiting:
             up = j > s
             behind = s - 1 if up else s + 1
-            if 0 <= behind < n and (s, j, e) not in arrival:
+            if 0 <= behind < n and (s, j, e) not in arrival and not direct(n, up, e):
                 continue
             start = max(term[s, j, e], clock[s], base[stage(n, s, j, e)])
             start = max(start, arrival.get((s, j, e), 0.0))
@@ -187,7 +191,8 @@
         up = j > s
         clock[s] = start + add
         links[s, up] = max(links.get((s, up), 0.0), start + add) + wire
-        arrival[s + 1 if up else s - 1, j, e] = links[s, up] + hop
+        if not direct(n, up, e):
+            arrival[s + 1 if up else s - 1, j, e] = links[s, up] + hop
     for s in range(n):
         tasks[s] += [(s, e) for e in COLUMN_ORDER[s]]
     return tasks
@@ -600,7 +605,7 @@
 
     for k, j in enumerate(row_order):
         if k == 2:
-            per_me(lambda s: hand_over(s, LAST_ROWS[s]))
+            per_me(lambda s: follow(s, LATE[s]))
         per_me(lambda s: rows_ready(ROW_ORDER[s][k]))
         piece = normed[j].reshape(rows, width)
         gate = jnp.dot(piece, wg_all[...], preferred_element_type=jnp.float32)
@@ -609,6 +614,7 @@
         down_part(j, column_order[0])
         if k:
             over_x(row_order[k - 1], column_order[0])
+    per_me(lambda s: down_arrived(s, COLUMN_ORDER[s][2]))
     over_x(row_order[-1], column_order[0])
 
     def local_sum(j, e):
@@ -629,12 +635,14 @@
 
     def over_z(s, j, e):
         acc = local_sum(j, e)
-        to = s + 1 if j > s else s - 1
-        behind = s - 1 if j > s else s + 1
-        if 0 <= behind < n:
-            acc += z_in(j, e)
+        if direct(n, j > s, e):
+            to, slot = j, n + 1 + s
+        else:
+            to = s + 1 if j > s else s - 1
+            slot = n if to == j and j < s else j
+            if 0 <= (s - 1 if j > s else s + 1) < n:
+                acc += z_in(j, e)
         z_send[j, :, span_of(e)] = acc.astype(jnp.bfloat16)
-        slot = n if to == j and j < s else j
 
         def make():
             return remote(
@@ -646,10 +654,12 @@
 
     def finish(s, e):
         acc = local_sum(s, e)
-        if s > 0:
-            acc += z_in(s, e)
-        if s < n - 1:
-            acc += z_in(n, e)
+        for up, others, slot in ((True, range(s), s), (False, range(s + 1, n), n)):
+            if direct(n, up, e):
+                for b in others:
+                    acc += z_in(n + 1 + b, e)
+            elif others:
+                acc += z_in(slot, e)
         total_ref[:, span_of(e)] = mixed[:, span_of(e)].astype(jnp.float32) + 0.5 * acc
 
     order = line_tasks(n)
@@ -671,7 +681,7 @@
         for j in row_order[::-1]:
             over_x(j, column_order[q])
         if q == 1:
-            per_me(lambda s: [down_arrived(s, e) for e in COLUMN_ORDER[s][2:]])
+            per_me(lambda s: down_arrived(s, COLUMN_ORDER[s][3]))
         if q < 3:
             per_me(lambda s: along(s, q - 1))
 
@@ -734,7 +744,7 @@
         ((n, nx, sub, width), bf16),
         ((n, nx, sub, width), bf16),
         ((n, sub, width), bf16),
-        ((n + 1, sub, width), bf16),
+        ((2 * n + 1, sub, width), bf16),
         ((sub, width), f32),
     ]
     sems = [
@@ -748,7 +758,7 @@
         (2, n, nx, PIECES),
         (2, n, n),
         (2, n, nx, n),
-        (2, n + 1, n),
+        (2, 2 * n + 1, n),
         (3,),
         (7,),
     ]

time: 107 us -> 101 us (0.944)
  Pallas kernels: 105 us -> 99.1 us
    pallas_call x1, Pallas kernels: 105 us -> 99.1 us  [fused_body(): pl.pallas_call(functools.partial(layer_kernel, n, tp, chunk), out_shape=j...]
where the time goes in v4:
time: 101 us
  Pallas kernels  99.1 us (98%)
  local copies, waits for them, and re-layouts  1.67 us (2%)
    pallas_call x1, Pallas kernels, fused_body(): pl.pallas_call(functools.partial(layer_kernel, n, tp, chunk), out_shape=j...  99.1 us

profile of v4, /device:TPU:0, one launch (start us, length us, event | category | flops | bytes accessed | tf_op | source)
XLA Modules:
  0.0 100.8 jit_solution(15155724813182809247)
XLA Ops:
  0.0 99.1 %shard_map.100 = bf16[64,2048]{1,0:T(8,128)(2,1)} custom-call(bf16[256,256]{1,0:T(8,128)(2,1)} %q_in.1, bf16[256,256]{1,0:T(8,128)(2,1)} %k_in.1, bf16[256,256]{1,0:T(8,128)(2,1)} %v_in.1, f32[4,256]{1,0:T(4,128)} %bitcast.3, bf16[256,2048]{1,0:T(8,128)(2,1)} %residual_in.1, bf16[256,2048]{1,0:T(8,128)(2,1)} %w_out_in.1, f32[1,2048]{1,0:T(1,128)} %bitcast.2, ...), custom_call_target="tpu_custom_call" | custom-call | tf_op jit(solution)/shard_map/pallas_call | solution.py:765
  99.1 1.7 %copy.12 = bf16[64,2048]{1,0:T(8,128)(2,1)} copy(bf16[64,2048]{1,0:T(8,128)(2,1)} %shard_map.100) | data formatting | bytes 524288

commit v5 on v4

--- a/solution.py
+++ b/solution.py
@@ -130,7 +130,7 @@
     ),
     (
         ("own",), ("fwd", 0), ("fwd", 3), ("hand", 1), ("fwd_dn", 0), ("in", 2), ("in", 0),
-        ("dn", 2, 3), ("in", 3), ("hand", 0), ("hand", 2),
+        ("dn", 2, 3), ("in", 3), ("hand", 2), ("hand", 0),
     ),
     (
         ("own",), ("fwd", 0), ("hand", 2), ("in", 3), ("dn", 1, 0), ("fwd_dn", 3), ("fwd", 1),
@@ -142,7 +142,7 @@
     ),
 )
 LATE = ((("hand", 3),), (("hand", 3),), (("hand", 0),), (("hand", 0),))
-STARTS = (2.0, 9.0, 16.5, 19.5)
+STARTS = (2.0, 9.5, 15.5, 19.5)
 
 
 def direct(n, up, e):

time: 101 us -> 101 us (level)
  no operation moved by 1% of the time
where the time goes in v5:
time: 101 us
  Pallas kernels  99.1 us (98%)
  local copies, waits for them, and re-layouts  1.67 us (2%)
    pallas_call x1, Pallas kernels, fused_body(): pl.pallas_call(functools.partial(layer_kernel, n, tp, chunk), out_shape=j...  99.1 us

profile of v5, /device:TPU:0, one launch (start us, length us, event | category | flops | bytes accessed | tf_op | source)
XLA Modules:
  0.0 100.8 jit_solution(10608770129259742791)
XLA Ops:
  0.0 99.1 %shard_map.100 = bf16[64,2048]{1,0:T(8,128)(2,1)} custom-call(bf16[256,256]{1,0:T(8,128)(2,1)} %q_in.1, bf16[256,256]{1,0:T(8,128)(2,1)} %k_in.1, bf16[256,256]{1,0:T(8,128)(2,1)} %v_in.1, f32[4,256]{1,0:T(4,128)} %bitcast.3, bf16[256,2048]{1,0:T(8,128)(2,1)} %residual_in.1, bf16[256,2048]{1,0:T(8,128)(2,1)} %w_out_in.1, f32[1,2048]{1,0:T(1,128)} %bitcast.2, ...), custom_call_target="tpu_custom_call" | custom-call | tf_op jit(solution)/shard_map/pallas_call | solution.py:765
  99.1 1.7 %copy.12 = bf16[64,2048]{1,0:T(8,128)(2,1)} copy(bf16[64,2048]{1,0:T(8,128)(2,1)} %shard_map.100) | data formatting | bytes 524288
